TPU v7x, 256 devices: a whole 4x4x8 slice. The times are simulated.
256 devices in a mesh: sp: 32 (over z, y), tp: 8 (over x, core).
Axes of the slice: x: 4, y: 4, z: 8, core: 2. Of those that a mesh axis runs over, the one named last changes fastest.
Arguments:
- hidden_states: bfloat16 [8192, 4096], P('sp', 'tp'), may hold values from -6 to 6
- norm_gain: float32 [4096], replicated, may hold values from 0.1 to 1.9
- query_weight: bfloat16 [4096, 2048], P('sp', 'tp'), may hold values from -0.09375 to 0.09375
- key_weight: bfloat16 [4096, 2048], P('sp', 'tp'), may hold values from -0.09375 to 0.09375
- value_weight: bfloat16 [4096, 2048], P('sp', 'tp'), may hold values from -0.09375 to 0.09375
- output_gate_weight: bfloat16 [4096, 2048], P('sp', 'tp'), may hold values from -0.09375 to 0.09375
- unit_input_weight: bfloat16 [4096, 2048], P('sp', 'tp'), may hold values from -0.09375 to 0.09375
- unit_gate_weight: bfloat16 [4096, 2048], P('sp', 'tp'), may hold values from -0.09375 to 0.09375
- decay_forward: float32 [16], P('tp'), may hold values from 0 to 16
- decay_backward: float32 [16], P('tp'), may hold values from 0 to 16
- group_gain: float32 [2048], P('tp'), may hold values from 0.1 to 1.9
- group_bias: float32 [2048], P('tp'), may hold values from -3 to 3
- depth_kernel: float32 [31, 2048], P(None, 'tp'), may hold values from -7 to 7
- depth_bias: float32 [2048], P('tp'), may hold values from -3 to 3
- channel_gain: float32 [2048], P('tp'), may hold values from 0.1 to 1.9
- channel_bias: float32 [2048], P('tp'), may hold values from -3 to 3
- retention_out_weight: bfloat16 [2048, 4096], P('tp', 'sp'), may hold values from -0.09375 to 0.09375
- convolution_out_weight: bfloat16 [2048, 4096], P('tp', 'sp'), may hold values from -0.09375 to 0.09375
Outputs:
- mixed_out: bfloat16 [8192, 4096], P(('sp', 'tp'))
All inputs are finite; a program needn't handle non-finite values.
Results may differ from a plain program's by a relative error of at most 0.018.
Values may be sent and summed in bfloat16 or wider, within the bound.
A program may use at most 128 MiB of HBM per device.

v0:
```python
import jax
import jax.numpy as jnp
from jax import lax
from jax.sharding import PartitionSpec as P

HEAD_DIM = 128
CONV_WIDTH = 2048
KERNEL = 31
BLOCK = 128


EPS = 1e-06
THETA = 10000.0


def in_order(blocks, dim):
    shape = list(blocks.shape[1:])
    shape[dim] *= blocks.shape[0]
    return jnp.moveaxis(blocks, 0, dim).reshape(shape)


def from_everyone(array, axis):
    count = lax.axis_size(axis)
    return lax.all_to_all(
        jnp.broadcast_to(array[None], (count, *array.shape)), axis, 0, 0, tiled=True
    )


def collect_2(array, axis, dim):
    return in_order(from_everyone(array, axis), dim)


def sent_together(arrays, axis, dim, along):
    widths = [a.shape[along] for a in arrays]
    both = jnp.concatenate(arrays, axis=along)
    result = lax.all_gather(both, axis, axis=dim, tiled=True)
    return tuple(jnp.split(result, [sum(widths[:k]) for k in range(1, len(widths))], axis=along))


def with_halo(cells, sides, width):
    for axis, dim in sides:
        count = lax.axis_size(axis)
        ends = count - 1
        head = lax.slice_in_dim(cells, 0, width, axis=dim)
        tail = lax.slice_in_dim(cells, cells.shape[dim] - width, cells.shape[dim], axis=dim)
        cells = jnp.concatenate(
            [
                lax.ppermute(tail, axis, [(i, (i + 1) % count) for i in range(ends)]),
                cells,
                lax.ppermute(head, axis, [((i + 1) % count, i) for i in range(ends)]),
            ],
            axis=dim,
        )
    return cells


def of_everyone(array, axis):
    everything = from_everyone(array, axis)
    return jnp.sum(everything, axis=0)


def in_one(arrays, axis):
    ends = [0]
    for a in arrays:
        ends.append(ends[-1] + a.size)
    subtotal = of_everyone(jnp.concatenate([a.ravel() for a in arrays]), axis)
    return tuple((subtotal[b:e].reshape(a.shape) for a, b, e in zip(arrays, ends, ends[1:])))


def split_up(array, dim, count):
    before, after = (array.shape[:dim], array.shape[dim + 1 :])
    return jnp.moveaxis(array.reshape(*before, count, -1, *after), dim, 0)


def sum_at_owner(array, axis, dim):
    blocks = split_up(array, dim, lax.axis_size(axis))
    arrived = lax.all_to_all(blocks, axis, split_axis=0, concat_axis=0, tiled=True)
    return arrived.astype(jnp.float32).sum(axis=0)


def rotate(rows, positions):
    half_dim = rows.shape[-1] // 2
    inverse = THETA ** (-jnp.arange(half_dim, dtype=jnp.float32) / half_dim)
    angles = positions.astype(jnp.float32)[:, None] * inverse[None, :]
    cosine = jnp.cos(angles)[:, None, :]
    sine = jnp.sin(angles)[:, None, :]
    widened = rows.astype(jnp.float32)
    first_half = widened[..., :half_dim]
    second_half = widened[..., half_dim:]
    turned = jnp.concatenate(
        [first_half * cosine - second_half * sine, second_half * cosine + first_half * sine],
        axis=-1,
    )
    return turned.astype(jnp.bfloat16)


def to_blocks(rows):
    return rows.reshape(rows.shape[0] // BLOCK, BLOCK, rows.shape[1], rows.shape[2]).transpose(
        2, 0, 1, 3
    )


def from_blocks(blocks):
    return blocks.transpose(1, 2, 0, 3).reshape(
        blocks.shape[1] * blocks.shape[2], blocks.shape[0], blocks.shape[3]
    )


def blockwise(queries, key_rows, values, log_decay, include_diag):
    block_len = queries.shape[2]
    position = jnp.arange(block_len, dtype=jnp.float32)
    distance = position[:, None] - position[None, :]
    allowed = distance >= 0 if include_diag else distance > 0
    inside = jnp.where(
        allowed[None], jnp.exp(log_decay[:, None, None] * jnp.maximum(distance, 0.0)[None]), 0.0
    )
    query_wide = queries.astype(jnp.float32)
    key_wide = key_rows.astype(jnp.float32)
    value_wide = values.astype(jnp.float32)
    scores = jnp.einsum("hnqd,hnkd->hnqk", query_wide, key_wide) * inside[:, None]
    inner_part = jnp.einsum("hnqk,hnkd->hnqd", scores, value_wide)
    toward_end = jnp.exp(log_decay[:, None] * (block_len - 1.0 - position)[None])
    block_states = jnp.einsum(
        "hnkd,hnke->hnde", key_wide * toward_end[:, None, :, None], value_wide
    )
    block_decay = jnp.exp(log_decay * block_len)[:, None, None]

    def advance(state_now, block_state):
        return (block_decay * state_now + block_state, state_now)

    initial = jnp.zeros(
        (block_states.shape[0], block_states.shape[2], block_states.shape[3]), jnp.float32
    )
    final_state, earlier = lax.scan(advance, initial, jnp.moveaxis(block_states, 1, 0))
    earlier = jnp.moveaxis(earlier, 0, 1)
    from_start = jnp.exp(log_decay[:, None] * (position + 1.0)[None])
    cross_part = jnp.einsum("hnqd,hnde->hnqe", query_wide * from_start[:, None, :, None], earlier)
    return (inner_part + cross_part, final_state)


def group_norm(retained, group_gain, group_bias, gate_rows):
    row_mean = jnp.mean(retained, axis=-1, keepdims=True)
    centered = retained - row_mean
    variance = jnp.mean(centered * centered, axis=-1, keepdims=True)
    scaled = (centered * lax.rsqrt(variance + EPS)).reshape(retained.shape[0], -1)
    scaled = scaled * group_gain[None, :] + group_bias[None, :]
    return (jax.nn.silu(gate_rows.astype(jnp.float32)) * scaled).astype(jnp.bfloat16)


def shards(
    hidden_states,
    norm_gain,
    query_weight,
    key_weight,
    value_weight,
    output_gate_weight,
    unit_input_weight,
    unit_gate_weight,
    decay_forward,
    decay_backward,
    group_gain,
    group_bias,
    depth_kernel,
    depth_bias,
    channel_gain,
    channel_bias,
    retention_out_weight,
    convolution_out_weight,
):
    row_total = hidden_states.shape[0]
    whole = collect_2(hidden_states, "tp", 1)
    widened = whole.astype(jnp.float32)
    normed = (
        widened
        * lax.rsqrt(jnp.mean(widened * widened, axis=-1, keepdims=True) + EPS)
        * norm_gain[None, :]
    ).astype(jnp.bfloat16)
    slabs = sent_together(
        (
            query_weight,
            key_weight,
            value_weight,
            output_gate_weight,
            unit_input_weight,
            unit_gate_weight,
        ),
        "sp",
        0,
        1,
    )
    summed = tuple((jnp.dot(normed, slab, preferred_element_type=jnp.float32) for slab in slabs))
    proj_q, proj_k, proj_v, proj_g, proj_a, proj_b = tuple(
        (part_sum.astype(jnp.bfloat16) for part_sum in summed)
    )
    head_count = proj_q.shape[1] // HEAD_DIM
    device = lax.axis_index("sp")
    positions = device * row_total + jnp.arange(row_total, dtype=jnp.int32)
    queries = rotate(proj_q.reshape(row_total, head_count, HEAD_DIM), positions)
    key_rows = rotate(proj_k.reshape(row_total, head_count, HEAD_DIM), positions)
    values = proj_v.reshape(row_total, head_count, HEAD_DIM)
    log_forward = jax.nn.log_sigmoid(decay_forward)
    log_backward = jax.nn.log_sigmoid(decay_backward)
    ahead_local, state_ahead = blockwise(
        to_blocks(queries), to_blocks(key_rows), to_blocks(values), log_forward, True
    )
    behind_local, state_behind = blockwise(
        to_blocks(queries[::-1]),
        to_blocks(key_rows[::-1]),
        to_blocks(values[::-1]),
        log_backward,
        False,
    )
    slabs = tuple(
        (
            part.astype(jnp.float32)
            for part in sent_together(
                (state_ahead[None].astype(jnp.bfloat16), state_behind[None].astype(jnp.bfloat16)),
                "sp",
                0,
                1,
            )
        )
    )
    source = jnp.arange(slabs[0].shape[0], dtype=jnp.int32)
    gap_ahead = device - 1 - source
    gap_behind = source - device - 1
    weight_ahead = jnp.where(
        gap_ahead[:, None] >= 0,
        jnp.exp(
            log_forward[None, :]
            * row_total
            * jnp.maximum(gap_ahead, 0).astype(jnp.float32)[:, None]
        ),
        0.0,
    )
    weight_behind = jnp.where(
        gap_behind[:, None] >= 0,
        jnp.exp(
            log_backward[None, :]
            * row_total
            * jnp.maximum(gap_behind, 0).astype(jnp.float32)[:, None]
        ),
        0.0,
    )
    enter_ahead = jnp.zeros_like(state_ahead) + jnp.einsum("jh,jhde->hde", weight_ahead, slabs[0])
    enter_behind = jnp.zeros_like(state_behind) + jnp.einsum(
        "jh,jhde->hde", weight_behind, slabs[1]
    )
    local_position = jnp.arange(row_total, dtype=jnp.float32)
    lift_ahead = jnp.exp(log_forward[None, :] * (local_position + 1.0)[:, None])
    lift_behind = jnp.exp(log_backward[None, :] * (row_total - local_position)[:, None])
    query_wide = queries.astype(jnp.float32)
    carried = jnp.einsum("shd,hde->she", query_wide * lift_ahead[:, :, None], enter_ahead)
    carried = carried + jnp.einsum(
        "shd,hde->she", query_wide * lift_behind[:, :, None], enter_behind
    )
    retained = from_blocks(ahead_local) + from_blocks(behind_local)[::-1] + carried
    retention_rows = group_norm(retained, group_gain, group_bias, proj_g)
    unit = (proj_a.astype(jnp.float32) * jax.nn.sigmoid(proj_b.astype(jnp.float32))).astype(
        jnp.bfloat16
    )
    half_kernel = (KERNEL - 1) // 2
    padded = with_halo(unit, (("sp", 0),), half_kernel)
    filtered = jnp.broadcast_to(depth_bias[None, :], (row_total, unit.shape[1]))
    for offset in range(KERNEL):
        filtered = filtered + depth_kernel[offset][None, :] * padded[
            offset : offset + row_total
        ].astype(jnp.float32)
    row_sum, row_squares = in_one(
        (jnp.sum(filtered, axis=1), jnp.sum(filtered * filtered, axis=1)), "tp"
    )
    row_mean = (row_sum / CONV_WIDTH)[:, None]
    variance = (row_squares / CONV_WIDTH)[:, None] - row_mean * row_mean
    leveled = (filtered - row_mean) * lax.rsqrt(variance + EPS) * channel_gain[
        None, :
    ] + channel_bias[None, :]
    convolution_rows = jax.nn.silu(leveled).astype(jnp.bfloat16)
    retention_full, convolution_full = sent_together(
        (retention_out_weight, convolution_out_weight), "sp", 1, 0
    )
    mixed = sum_at_owner(
        (
            jnp.dot(retention_rows, retention_full, preferred_element_type=jnp.float32)
            + jnp.dot(convolution_rows, convolution_full, preferred_element_type=jnp.float32)
        ).astype(jnp.bfloat16),
        "tp",
        0,
    )
    return mixed.astype(jnp.bfloat16)


def solution(mesh):
    placed = (
        P("sp", "tp"),
        P(),
        P("sp", "tp"),
        P("sp", "tp"),
        P("sp", "tp"),
        P("sp", "tp"),
        P("sp", "tp"),
        P("sp", "tp"),
        P("tp"),
        P("tp"),
        P("tp"),
        P("tp"),
        P(None, "tp"),
        P("tp"),
        P("tp"),
        P("tp"),
        P("tp", "sp"),
        P("tp", "sp"),
    )
    return jax.shard_map(
        shards, mesh=mesh, in_specs=placed, out_specs=P(("sp", "tp"), None), check_vma=False
    )
```

profile of v0, /device:TPU:1, one launch (start us, length us, event | category | flops | bytes accessed | tf_op | source)
XLA Modules:
  0.0 365.9 jit_solution(17204845158088076287)
XLA Ops:
  6.5 0.8 constant_dynamic-update-slice_fusion.5
  7.4 0.8 constant_dynamic-update-slice_fusion.4
  8.2 0.8 constant_dynamic-update-slice_fusion.3
  9.1 0.8 constant_dynamic-update-slice_fusion.2
  9.9 0.8 constant_dynamic-update-slice_fusion.1
  10.8 0.8 constant_dynamic-update-slice_fusion
  11.6 0.7 copy-done.1
  12.4 1.1 copy.86
  13.5 1.5 broadcast_in_dim.49
  14.9 6.8 %all-to-all-start = ((bf16[8,256,512]{1,2,0:T(8,128)(2,1)}), bf16[8,256,512]{1,2,0:T(8,128)(2,1)S(1)}, u32[]{:S(2)}, u32[]{:S(2)}) async-start(bf16[8,256,512]{1,2,0:T(8,128)(2,1)} %broadcast_in_dim.49), calls=%async_computation | async-start | bytes 4194304 | tf_op jit(solution)/shard_map/all_to_all | solution.py:24
  22.5 0.7 multiply_exponential_fusion.3
  23.1 1.2 multiply_cosine_fusion
  24.3 23.7 %all-to-all-done = bf16[8,256,512]{1,2,0:T(8,128)(2,1)S(1)} async-done(((bf16[8,256,512]{1,2,0:T(8,128)(2,1)}), bf16[8,256,512]{1,2,0:T(8,128)(2,1)S(1)}, u32[]{:S(2)}, u32[]{:S(2)}) %all-to-all-start) | async-done | bytes 2097184 | tf_op jit(solution)/shard_map/all_to_all | solution.py:24
  48.0 0.6 multiply_reduce_fusion.2
  48.6 1.7 fusion.2
  50.3 84.2 %all-gather.4.cloned.1.call-done = bf16[4096,1536]{1,0:T(8,128)(2,1)} async-done(((bf16[128,1536]{1,0:T(8,128)(2,1)}), bf16[4096,1536]{1,0:T(8,128)(2,1)}) %all-gather.4.cloned.1.call-update) | async-done | bytes 12582928 | tf_op jit(solution)/shard_map/all_gather | solution.py:36
  134.5 3.1 fusion.28
  137.9 2.5 fusion.31
  140.5 0.8 copy.130
  141.3 0.9 copy.131
  142.2 1.2 subtract_convert_fusion.1
  143.7 2.5 fusion.34
  146.2 0.7 reshape_reshape.3
  147.6 0.8 convolution_bitcast_fusion
  148.4 0.7 broadcast.372.clone
  149.1 1.5 while.27
  149.1 0.6 bitcast_dynamic-update-slice_fusion.5
  149.8 0.6 bitcast_dynamic-update-slice_fusion.5
  150.6 1.0 copy.91
  151.6 0.9 convolution_bitcast_fusion.1
  152.5 0.7 broadcast.372.clone.1
  153.2 1.4 while.26
  153.2 0.6 bitcast_dynamic-update-slice_fusion.4
  153.9 0.6 bitcast_dynamic-update-slice_fusion.4
  154.7 0.7 pad_maximum_fusion.4
  155.5 1.5 pad_maximum_fusion.5
  157.2 0.7 multiply_exponential_fusion.1
  157.9 0.6 multiply_exponential_fusion
  158.5 0.7 select_bitcast_fusion.1
  159.2 1.3 select_bitcast_fusion
  160.5 1.6 fusion.149
  162.1 1.7 fusion.148
  163.8 1.5 exponential_select_fusion
  165.3 2.4 fusion.64
  167.7 2.3 fusion.46
  170.1 0.6 fusion.145
  170.7 2.4 collective-permute-start
  173.1 1.3 collective-permute-start.1
  174.7 1.2 fusion.20
  176.0 1.1 convolution_add_fusion.2
  177.1 2.0 fusion.21
  179.1 6.3 %fusion.142 = (f32[256]{0:T(256)S(1)}, f32[256]{0:T(256)S(1)}, f32[256,256]{1,0:T(8,128)S(1)}) fusion(bf16[15,256]{1,0:T(8,128)(2,1)} %collective-permute-done.1, bf16[256,256]{1,0:T(8,128)(2,1)} %copy-done.2, f32[256]{0:T(256)} %bitcast.198, f32[256]{0:T(256)} %bitcast.199, f32[256]{0:T(256)} %bitcast.201, f32[256]{0:T(256)} %bitcast.202, ...), kind=kLoop, calls=%fused_computation.233 | loop fusion | flops 12189184 | bytes 443392 | tf_op jit(solution)/shard_map/reduce_sum | solution.py:270
  185.4 0.6 broadcast_in_dim.63
  186.0 5.9 %all-to-all-start.1 = ((f32[8,1,512]{2,1,0:T(1,128)}), f32[8,1,512]{2,1,0:T(1,128)S(1)}, u32[]{:S(2)}, u32[]{:S(2)}) async-start(f32[8,1,512]{2,1,0:T(1,128)} %broadcast_in_dim.63), calls=%async_computation.1 | async-start | bytes 32768 | tf_op jit(solution)/shard_map/all_to_all | solution.py:24
  191.9 2.0 convolution_add_fusion.3
  194.4 1.1 copy.101
  195.5 1.1 all-to-all-done.1
  196.7 35.0 %all-gather.6.cloned.1.call-done = bf16[32,4,128,128]{3,2,1,0:T(8,128)(2,1)} async-done(((bf16[1,4,128,128]{3,2,1,0:T(8,128)(2,1)}), bf16[32,4,128,128]{3,2,1,0:T(8,128)(2,1)}) %all-gather.6.cloned.1.call-update) | async-done | bytes 4194320 | tf_op jit(solution)/shard_map/all_gather | solution.py:36
  231.7 3.1 multiply_reduce_fusion
  235.7 78.7 %all-gather.8.cloned.1.call-done = bf16[512,4096]{1,0:T(8,128)(2,1)} async-done(((bf16[512,128]{1,0:T(8,128)(2,1)}), bf16[512,4096]{1,0:T(8,128)(2,1)}) %all-gather.8.cloned.1.call-update) | async-done | bytes 4194320 | tf_op jit(solution)/shard_map/all_gather | solution.py:36
  314.4 6.6 %fusion.8 = f32[256,4096]{1,0:T(8,128)} fusion(bf16[512,4096]{1,0:T(8,128)(2,1)} %all-gather.8.cloned.1.call-done, f32[256,256]{1,0:T(8,128)S(1)} %copy.124, bf16[256,4096]{0,1:T(8,128)(2,1)S(1)} %copy-done, bf16[4096,1536]{1,0:T(8,128)(2,1)} %all-gather.4.cloned.1.call-done, f32[256]{0:T(256)S(1)} %copy-done.9, f32[256]{0:T(256)S(1)} %copy-done.10), kind=kOutput, calls=%fused_computation.17 | convolution fusion | flops 1074397184 | bytes 10749952 | tf_op jit(solution)/shard_map/dot_general | solution.py:283
  321.0 3.6 fusion
  324.6 33.7 %all_to_all.16 = bf16[8,32,4096]{2,1,0:T(8,128)(2,1)S(1)} all-to-all(bf16[8,32,4096]{2,1,0:T(8,128)(2,1)S(1)} %bitcast.165), channel_id=1, replica_groups=mesh['sp'=32,'tp'=8] {'tp'}, dimensions={0} | all-to-all | bytes 4194304 | tf_op jit(solution)/shard_map/all_to_all | solution.py:77
  358.3 1.1 reduce_sum.72
  (83 shorter events, 4.1 us)
Async XLA Ops:
  6.5 127.9 %all-gather.4.cloned.1.call-start = ((), (), s32[]{:S(2)}) async-start(), calls=%async_computation.3 | async-start | bytes 12976128 | tf_op jit(solution)/shard_map/all_gather | solution.py:36
  11.6 0.7 copy-start.1
  14.9 6.9 %copy-start.13 = (f32[2]{0:T(128)S(1)}, f32[2]{0:T(128)}, u32[]{:S(2)}) copy-start(f32[2]{0:T(128)} %param.31) | copy-start | bytes 28
  14.9 6.9 %copy-start.14 = (f32[2]{0:T(128)S(1)}, f32[2]{0:T(128)}, u32[]{:S(2)}) copy-start(f32[2]{0:T(128)} %param.30) | copy-start | bytes 28
  14.9 33.1 %all-to-all-start = ((bf16[8,256,512]{1,2,0:T(8,128)(2,1)}), bf16[8,256,512]{1,2,0:T(8,128)(2,1)S(1)}, u32[]{:S(2)}, u32[]{:S(2)}) async-start(bf16[8,256,512]{1,2,0:T(8,128)(2,1)} %broadcast_in_dim.49), calls=%async_computation | async-start | bytes 4194304 | tf_op jit(solution)/shard_map/all_to_all | solution.py:24
  21.8 26.8 %copy-start.4 = (f32[4096]{0:T(1024)S(1)}, f32[4096]{0:T(1024)}, u32[]{:S(2)}) copy-start(f32[4096]{0:T(1024)} %param.23) | copy-start | bytes 49156
  21.8 209.9 %all-gather.6.cloned.1.call-start = ((), (), s32[]{:S(2)}) async-start(), calls=%async_computation.4 | async-start | bytes 4325376 | tf_op jit(solution)/shard_map/all_gather | solution.py:36
  22.4 134.7 %copy-start.8 = (f32[2]{0:T(128)}, f32[2]{0:T(128)S(1)}, u32[]{:S(2)}) copy-start(f32[2]{0:T(128)S(1)} %get-tuple-element.238) | copy-start | bytes 28
  22.4 135.4 %copy-start.7 = (f32[2]{0:T(128)}, f32[2]{0:T(128)S(1)}, u32[]{:S(2)}) copy-start(f32[2]{0:T(128)S(1)} %get-tuple-element.179) | copy-start | bytes 28
  50.3 87.6 %copy-start = (bf16[256,4096]{0,1:T(8,128)(2,1)S(1)}, bf16[256,4096]{0,1:T(8,128)(2,1)}, u32[]{:S(2)}) copy-start(bf16[256,4096]{0,1:T(8,128)(2,1)} %fusion.2) | copy-start | bytes 6291460
  155.4 159.0 %all-gather.8.cloned.1.call-start = ((), (), s32[]{:S(2)}) async-start(), calls=%async_computation.5 | async-start | bytes 4325376 | tf_op jit(solution)/shard_map/all_gather | solution.py:36
  170.0 4.4 %copy-start.2 = (bf16[256,256]{1,0:T(8,128)(2,1)}, bf16[256,256]{1,0:T(8,128)(2,1)S(1)}, u32[]{:S(2)}) copy-start(bf16[256,256]{1,0:T(8,128)(2,1)S(1)} %fusion.46) | copy-start | bytes 393220
  170.7 8.4 %collective-permute-start = (bf16[15,256]{1,0:T(8,128)(2,1)}, bf16[15,256]{1,0:T(8,128)(2,1)}, u32[]{:S(2)}, u32[]{:S(2)}) collective-permute-start(bf16[15,256]{1,0:T(8,128)(2,1)} %get-tuple-element.186), channel_id=1, source_target_pairs={{0,8},{8,16},{16,24},{24,32},{32,40},{40,48},{48,56},{56,64},{64,7... | collective-permute-start | bytes 23048 | tf_op jit(solution)/shard_map/ppermute | solution.py:48
  173.1 6.0 %collective-permute-start.1 = (bf16[15,256]{1,0:T(8,128)(2,1)}, bf16[15,256]{1,0:T(8,128)(2,1)}, u32[]{:S(2)}, u32[]{:S(2)}) collective-permute-start(bf16[15,256]{1,0:T(8,128)(2,1)} %get-tuple-element.187), channel_id=1, source_target_pairs={{8,0},{16,8},{24,16},{32,24},{40,32},{48,40},{56,48},{64,56},{72,6... | collective-permute-start | bytes 23048 | tf_op jit(solution)/shard_map/ppermute | solution.py:50
  179.1 52.6 %copy-start.3 = (f32[2,32]{0,1:T(8,128)S(1)}, f32[2,32]{0,1:T(8,128)}, u32[]{:S(2)}) copy-start(f32[2,32]{0,1:T(8,128)} %select_bitcast_fusion) | copy-start | bytes 772
  186.0 10.6 %all-to-all-start.1 = ((f32[8,1,512]{2,1,0:T(1,128)}), f32[8,1,512]{2,1,0:T(1,128)S(1)}, u32[]{:S(2)}, u32[]{:S(2)}) async-start(f32[8,1,512]{2,1,0:T(1,128)} %broadcast_in_dim.63), calls=%async_computation.1 | async-start | bytes 32768 | tf_op jit(solution)/shard_map/all_to_all | solution.py:24
  196.6 38.2 %copy-start.6 = (f32[256,2]{0,1:T(2,128)S(1)}, f32[256,2]{0,1:T(2,128)}, u32[]{:S(2)}) copy-start(f32[256,2]{0,1:T(2,128)} %multiply_exponential_fusion.1) | copy-start | bytes 6148
  196.6 38.5 %copy-start.5 = (f32[256,2]{0,1:T(2,128)S(1)}, f32[256,2]{0,1:T(2,128)}, u32[]{:S(2)}) copy-start(f32[256,2]{0,1:T(2,128)} %multiply_exponential_fusion) | copy-start | bytes 6148
  234.8 79.6 %copy-start.9 = (f32[256]{0:T(256)S(1)}, f32[256]{0:T(256)}, u32[]{:S(2)}) copy-start(f32[256]{0:T(256)} %param.33) | copy-start | bytes 3076
  234.8 79.6 %copy-start.10 = (f32[256]{0:T(256)S(1)}, f32[256]{0:T(256)}, u32[]{:S(2)}) copy-start(f32[256]{0:T(256)} %param.32) | copy-start | bytes 3076
  235.7 85.3 %copy-start.11 = (f32[256]{0:T(256)S(1)}, f32[256]{0:T(256)}, u32[]{:S(2)}) copy-start(f32[256]{0:T(256)} %param.37) | copy-start | bytes 3076
  235.7 85.3 %copy-start.12 = (f32[256]{0:T(256)S(1)}, f32[256]{0:T(256)}, u32[]{:S(2)}) copy-start(f32[256]{0:T(256)} %param.36) | copy-start | bytes 3076
Sparse Core Ops, SparseCore 0:
  12.5 121.9 all-gather.3
  155.5 76.0 all-gather.5
  234.1 80.2 all-gather.7
where the time goes:
time: 368 us; the launch traced here: 366 us
  waiting for transfers between devices  223 us (61%)
  blocking collectives  33.7 us (9%)
  matrix products  31.8 us (9%)
  other arithmetic  26.8 us (7%)
  local copies, waits for them, and re-layouts  20.8 us (6%)
  starting transfers between devices  16.5 us (4%)
  between operations  13.6 us (4%)
    all_gather x3, waiting for transfers between devices, sent_together(): result = lax.all_gather(both, axis, axis=dim, tiled=True)  198 us
    all_to_all x1, blocking collectives, sum_at_owner(): lax.all_to_all(blocks, axis, split_axis=0, concat_axis=0, tiled=True)  33.7 us
    all_to_all x2, waiting for transfers between devices, from_everyone(): lax.all_to_all(jnp.broadcast_to(array[None], (count, *array.shape)), axis...  24.8 us
    dot_general x5, matrix products, shards(): jnp.dot(normed, slab, preferred_element_type=jnp.float32)  12.9 us
    all_to_all x2, starting transfers between devices, from_everyone(): lax.all_to_all(jnp.broadcast_to(array[None], (count, *array.shape)), axis...  12.8 us
    unnamed x40, local copies, waits for them, and re-layouts  8.06 us
  transfers between devices with their start and end apart: 7, of which 5 were waited for; matrix products, arithmetic and copies ran while one was open for 11% of the time, Pallas kernels for 0%

commit v1 on v0

v1 whole, which is shorter than its diff:
```python
import functools

import jax
import jax.numpy as jnp
from jax import lax
from jax.experimental import pallas as pl
from jax.experimental.pallas import tpu as pltpu
from jax.sharding import PartitionSpec as P

HEAD_DIM = 128
CONV_WIDTH = 2048
KERNEL = 31
EPS = 1e-06
THETA = 10000.0
ROWS = 512
BF = jnp.bfloat16
F32 = jnp.float32
MESH = pl.DeviceIdType.MESH
VM = pl.BlockSpec(memory_space=pltpu.VMEM)
ANY = pl.BlockSpec(memory_space=pl.ANY)
MIB = 1 << 20


def place():
    sp, tp = lax.axis_index("sp"), lax.axis_index("tp")
    return tp // 2, sp % 4, sp // 4, tp % 2


def at(x, y, z, c):
    return (z * 4 + y, x * 2 + c)


def when(cond, f):
    if cond is None:
        f()
    else:
        pl.when(cond)(f)


class Post:
    def __init__(self, send_sems, recv_sems):
        self.ss, self.rs = send_sems, recv_sems
        self.sent, self.ids = [], {}

    def key(self, name):
        return self.rs.at[self.ids.setdefault(name, len(self.ids))]

    def send(self, name, src, dst, to, cond=None):
        sem, recv = self.ss.at[len(self.sent)], self.key(name)

        def make():
            return pltpu.make_async_remote_copy(
                src_ref=src, dst_ref=dst, send_sem=sem, recv_sem=recv, device_id=to, device_id_type=MESH
            )

        self.sent.append((make, cond))
        when(cond, lambda: make().start())

    def local(self, name, src, dst, cond=None):
        recv = self.key(name)
        when(cond, lambda: pltpu.make_async_copy(src, dst, recv).start())

    def recv(self, name, ref, cond=None):
        recv = self.key(name)
        when(cond, lambda: pltpu.make_async_copy(ref, ref, recv).wait())

    def finish(self):
        for make, cond in self.sent:
            when(cond, lambda: make().wait_send())


def greet(peers):
    barrier = pltpu.get_barrier_semaphore()
    for peer in peers:
        pl.semaphore_signal(barrier, inc=1, device_id=peer, device_id_type=MESH)
    pl.semaphore_wait(barrier, len(peers))


def rows_at(start, size, unit=16):
    return pl.ds(pl.multiple_of(start, unit), size)


def cols_at(start, size):
    return pl.ds(pl.multiple_of(start, 128), size)


def gather_kernel(xin, wq, wk, wv, wg, wa, wb, wr, wc, par, xg, wt, wo, pg, ss, rs):
    x, y, z, c = place()
    ct, yl = y // 2, y % 2
    xp, xm, x2 = (x + 1) % 4, (x + 3) % 4, (x + 2) % 4
    yp, ym, y2 = (y + 1) % 4, (y + 3) % 4, (y + 2) % 4
    zp, zm = (z + 1) % 8, (z + 7) % 8
    own = ct == c
    other = ct != c
    post = Post(ss, rs)
    partner = at(x, y, z, 1 - c)
    greet(
        [at(q, y, z, k) for q in (xp, xm) for k in (0, 1)]
        + [at(x, q, z, k) for q in (yp, ym, y2) for k in (0, 1)]
        + [at(x, y, zp, c), at(x, y, zm, c), partner]
    )

    def xblock(yy, half, r0, rn, col, width):
        return xg.at[rows_at((yy % 2) * 256 + half * 128 + r0, rn), cols_at(col, width)]

    mine = (x * 2 + c) * 512
    for half, name, ends in ((0, "x1", ((xp, y, "m"), (xm, y, "p"))), (1, "x2", ((x, yp, "m"), (x, ym, "p")))):
        src, dst = xin.at[pl.ds(half * 128, 128), :], xblock(y, half, 0, 128, mine, 512)
        for qx, qy, d in ends:
            post.send(name + d, src, dst, at(qx, qy, z, ct))
        post.send(name + "l", src, dst, partner, other)
        post.local(name + "s", src, dst, own)

    s = z * 4 + y
    for j in (0, 1):
        q = 2 * c + j
        here = (q == y) & own
        away = jnp.logical_not(here)
        to = at(x, q, z, ct)
        for m, w in enumerate((wq, wk, wv, wg, wa, wb)):
            src, dst = w.at[:, pl.ds(j * 128, 128)], wt.at[rows_at(s * 128, 128), pl.ds(m * 128, 128)]
            post.send("w", src, dst, to, away)
            post.local("w", src, dst, here)
    for j in (0, 1):
        q = 2 * c + j
        here = (q == y) & own
        away = jnp.logical_not(here)
        to = at(x, q, z, ct)
        for m, w in enumerate((wr, wc)):
            src, dst = w.at[pl.ds(j * 128, 128), :], wo.at[pl.ds(m * 128, 128), cols_at(s * 128, 128)]
            post.send("o", src, dst, to, away)
            post.local("o", src, dst, here)
    src = par.at[:, cols_at(yl * 128, 128)]
    post.send("par", src, pg, partner, own)
    post.local("pars", src, pg, own)

    def wrows(zz, u, n=1):
        return wt.at[rows_at((zz * 4 + 2 * c + u) * 128, 128 * n), :]

    def zsend(zz, u, r, d):
        ref = wrows(zz, u)
        post.send(("z", d, r, u), ref, ref, at(x, y, zp if d == "m" else zm, c))

    def zpass(zz, u, rel):
        ref = wrows(zz, u)
        post.send(("zp", rel, u), ref, ref, partner)

    def ocols(zz, core=c, r0=0, rn=256):
        return wo.at[pl.ds(r0, rn), cols_at((zz * 4 + 2 * core) * 128, 256)]

    def osend(zz, r, d, r0=0, rn=256):
        ref = ocols(zz, c, r0, rn)
        post.send(("o", d, r), ref, ref, at(x, y, zp if d == "m" else zm, c))

    def opass(zz, rel, r0=0, rn=256):
        ref = ocols(zz, c, r0, rn)
        post.send(("op", rel, r0), ref, ref, partner)

    post.recv("w", wrows(z, 0, 2))
    for d, order in (("m", (0, 1)), ("p", (1, 0))):
        for u in order:
            zsend(z, u, 1, d)
    for u in (0, 1):
        zpass(z, u, 0)

    cm, cp, c2 = ym // 2 == c, yp // 2 == c, y2 // 2 == c
    post.recv("x1m", xblock(y, 0, 0, 128, xm * 1024, 1024), own)
    ref = xblock(y, 0, 0, 64, xm * 1024, 1024)
    post.send("x1m2", ref, ref, at(xp, y, z, c), own)
    post.recv("x1p", xblock(y, 0, 0, 128, xp * 1024, 1024), own)
    ref = xblock(y, 0, 64, 64, xp * 1024, 1024)
    post.send("x1p2", ref, ref, at(xm, y, z, c), own)
    post.recv("x2m", xblock(ym, 1, 0, 128, x * 1024, 1024), cm)
    ref = xblock(ym, 1, 0, 64, x * 1024, 1024)
    post.send("x2m2", ref, ref, at(x, yp, z, c), cm)
    post.recv("x2p", xblock(yp, 1, 0, 128, x * 1024, 1024), cp)
    ref = xblock(yp, 1, 64, 64, x * 1024, 1024)
    post.send("x2p2", ref, ref, at(x, ym, z, c), cp)

    for name, half in (("x1", 0), ("x2", 1)):
        block = xblock(y, half, 0, 128, mine, 512)
        post.recv(name + "s", block, own)
        post.recv(name + "l", xblock(y, half, 0, 128, (x * 2 + 1 - c) * 512, 512), own)
    post.recv("x1m2", xblock(y, 0, 0, 64, x2 * 1024, 1024), own)
    post.recv("x1p2", xblock(y, 0, 64, 64, x2 * 1024, 1024), own)
    for u in (0, 1):
        ref = xblock(y, 0, u * 64, 64, 0, 4096)
        post.send(("x3m", u), ref, ref, at(x, yp, z, c), own)
    for u in (1, 0):
        ref = xblock(y, 0, u * 64, 64, 0, 4096)
        post.send(("x3p", u), ref, ref, at(x, ym, z, c), own)
    post.recv("x2m2", xblock(y2, 1, 0, 64, x * 1024, 1024), c2)
    post.recv("x2p2", xblock(y2, 1, 64, 64, x * 1024, 1024), c2)

    def x4(qx, k):
        return xblock(k, 1, 0, 128, qx * 1024, 1024)

    for d, to, order in (("m", xp, (0, 1)), ("p", xm, (1, 0))):
        for k in order:
            post.send(("x4" + d, k), x4(x, k), x4(x, k), at(to, y, z, c))

    def zstep(r):
        for i in (0, 1):
            for d, u in (("m", i), ("p", 1 - i)):
                zz = (z - r) % 8 if d == "m" else (z + r) % 8
                post.recv(("z", d, r, u), wrows(zz, u))
                if r < 3 or i == 0:
                    zsend(zz, u, r + 1, d)
                zpass(zz, u, -r % 8 if d == "m" else r)

    zstep(1)
    post.recv(("x3m", 0), xblock(ym, 0, 0, 64, 0, 4096), cm)
    ref = xblock(ym, 0, 0, 64, 0, 4096)
    post.send("x3m2", ref, ref, at(x, yp, z, c), cm)
    post.recv(("x3p", 1), xblock(yp, 0, 64, 64, 0, 4096), cp)
    ref = xblock(yp, 0, 64, 64, 0, 4096)
    post.send("x3p2", ref, ref, at(x, ym, z, c), cp)
    post.recv(("x4m", 0), x4(xm, 0))
    post.send("x4m2", x4(xm, 0), x4(xm, 0), at(xp, y, z, c))
    post.recv(("x4p", 1), x4(xp, 1))
    post.send("x4p2", x4(xp, 1), x4(xp, 1), at(xm, y, z, c))
    zstep(2)
    post.recv("o", ocols(z))
    zstep(3)
    for d in ("m", "p"):
        osend(z, 1, d)
    opass(z, 0)
    for d, u in (("m", 0), ("p", 1)):
        post.recv(("z", d, 4, u), wrows((z + 4) % 8, u))
        zpass((z + 4) % 8, u, 4)
    for r in (1, 2, 3):
        for d in ("m", "p"):
            zz = (z - r) % 8 if d == "m" else (z + r) % 8
            post.recv(("o", d, r), ocols(zz))
            if r < 3:
                osend(zz, r + 1, d)
            else:
                osend(zz, 4, d, 0 if d == "m" else 128, 128)
            opass(zz, -r % 8 if d == "m" else r)
    for d, r0 in (("m", 0), ("p", 128)):
        post.recv(("o", d, 4), ocols((z + 4) % 8, c, r0, 128))
        opass((z + 4) % 8, 4, r0, 128)

    post.recv("pars", pg, own)
    post.recv("par", pg, other)
    post.recv(("x3m", 1), xblock(ym, 0, 64, 64, 0, 4096), cm)
    post.recv(("x3p", 0), xblock(yp, 0, 0, 64, 0, 4096), cp)
    post.recv("x3m2", xblock(y2, 0, 0, 64, 0, 4096), c2)
    post.recv("x3p2", xblock(y2, 0, 64, 64, 0, 4096), c2)
    post.recv(("x4m", 1), x4(xm, 1))
    post.recv(("x4p", 0), x4(xp, 0))
    post.recv("x4m2", x4(x2, 0))
    post.recv("x4p2", x4(x2, 1))
    for rel in range(8):
        zz = (z + rel) % 8
        for u in (0, 1):
            ref = wt.at[rows_at((zz * 4 + 2 * (1 - c) + u) * 128, 128), :]
            post.recv(("zp", rel, u), ref)
        if rel == 4:
            for r0 in (0, 128):
                post.recv(("op", rel, r0), ocols(zz, 1 - c, r0, 128))
        else:
            post.recv(("op", rel, 0), ocols(zz, 1 - c))
    post.finish()


def gather(xin, weights, outs, par):
    return pl.pallas_call(
        gather_kernel,
        name="gather",
        out_shape=(
            jax.ShapeDtypeStruct((ROWS, 4096), BF),
            jax.ShapeDtypeStruct((4096, 768), BF),
            jax.ShapeDtypeStruct((256, 4096), BF),
            jax.ShapeDtypeStruct((40, 128), F32),
        ),
        in_specs=[ANY] * 10,
        out_specs=(VM,) * 4,
        scratch_shapes=[pltpu.SemaphoreType.DMA((128,)), pltpu.SemaphoreType.DMA((96,))],
        compiler_params=pltpu.CompilerParams(
            collective_id=0, has_side_effects=True, vmem_limit_bytes=32 * MIB
        ),
    )(xin, *weights, *outs, par)


def dot(a, b, dims=((1,), (0,))):
    return lax.dot_general(a, b, (dims, ((), ())), preferred_element_type=F32)


def project_kernel(xg, wt, pg, gain, cosine, sine, q_ref, in_ref, g_ref, u_ref, st_ref, nrm):
    @pl.loop(0, ROWS // 128)
    def _(i):
        rows = rows_at(i * 128, 128)
        square = jnp.zeros((128, 128), F32)
        for k in range(32):
            part = xg[rows, k * 128 : k * 128 + 128].astype(F32)
            square = square + part * part
        scale = lax.rsqrt(jnp.sum(square, axis=1, keepdims=True) / 4096 + EPS)
        for k in range(32):
            cols = slice(k * 128, k * 128 + 128)
            nrm[rows, cols] = (xg[rows, cols].astype(F32) * scale * gain[:, cols]).astype(BF)

    proj = dot(nrm[...], wt[...]).astype(BF)

    def turn(rows):
        wide = rows.astype(F32)
        return (wide * cosine[...] + pltpu.roll(wide, 64, axis=1) * sine[...]).astype(BF)

    queries, keys = turn(proj[:, 0:128]), turn(proj[:, 128:256])
    values = proj[:, 256:384]
    q_ref[...] = queries
    g_ref[...] = proj[:, 384:512]
    u_ref[...] = (proj[:, 512:640].astype(F32) * jax.nn.sigmoid(proj[:, 640:768].astype(F32))).astype(BF)
    lf, lb = pg[36:37, :], pg[37:38, :]
    place_ = lax.broadcasted_iota(jnp.int32, (ROWS, 128), 0).astype(F32)
    wide = keys.astype(F32)
    st_ref[0] = dot((wide * jnp.exp(lb * place_)).astype(BF), values, ((0,), (0,))).astype(BF)
    st_ref[1] = dot((wide * jnp.exp(lf * (ROWS - 1.0 - place_))).astype(BF), values, ((0,), (0,))).astype(BF)
    f1, b1 = lf[:, 0:1], lb[:, 0:1]
    for i in range(ROWS // 128):
        rows = slice(i * 128, i * 128 + 128)
        gap = (
            lax.broadcasted_iota(jnp.int32, (128, ROWS), 0)
            + i * 128
            - lax.broadcasted_iota(jnp.int32, (128, ROWS), 1)
        ).astype(F32)
        decay = jnp.exp(jnp.where(gap >= 0, f1 * gap, -b1 * gap))
        scores = dot(queries[rows], keys, ((1,), (1,))) * decay
        in_ref[rows, :] = dot(scores.astype(BF), values)


def project(xg, wt, pg, gain, cosine, sine):
    small = jax.ShapeDtypeStruct((ROWS, 128), BF)
    return pl.pallas_call(
        project_kernel,
        name="project",
        out_shape=(
            small,
            jax.ShapeDtypeStruct((ROWS, 128), F32),
            small,
            small,
            jax.ShapeDtypeStruct((2, 128, 128), BF),
        ),
        in_specs=[VM] * 6,
        out_specs=(VM,) * 5,
        scratch_shapes=[pltpu.VMEM((ROWS, 4096), BF)],
        compiler_params=pltpu.CompilerParams(vmem_limit_bytes=40 * MIB),
    )(xg, wt, pg, gain, cosine, sine)


def states_kernel(st, unit, sg, halo, ss, rs):
    x, y, z, c = place()
    n = z * 2 + c
    post = Post(ss, rs)
    peers = []
    for dz in range(8):
        for k in (0, 1):
            if dz or k:
                n2 = ((z + dz) % 8) * 2 + (c + k) % 2
                peers.append((n2, at(x, y, n2 // 2, n2 % 2)))
    greet([peer for _, peer in peers])
    after, before = (n + 1) % 16, (n + 15) % 16
    post.send("ht", unit.at[pl.ds(ROWS - 16, 16), :], halo.at[0], at(x, y, after // 2, after % 2))
    post.send("hh", unit.at[pl.ds(0, 16), :], halo.at[1], at(x, y, before // 2, before % 2))
    for n2, peer in peers:
        post.send("st", st.at[(n2 - n + 16) // 16], sg.at[n], peer)
    sg[pl.ds(n, 1)] = jnp.zeros((1, 128, 128), BF)
    post.recv("ht", halo.at[0])
    post.recv("hh", halo.at[1])
    post.recv("st", sg.at[pl.ds(0, 15)])
    post.finish()


def exchange_states(st, unit):
    return pl.pallas_call(
        states_kernel,
        name="states",
        out_shape=(jax.ShapeDtypeStruct((16, 128, 128), BF), jax.ShapeDtypeStruct((2, 16, 128), BF)),
        in_specs=[VM] * 2,
        out_specs=(VM,) * 2,
        scratch_shapes=[pltpu.SemaphoreType.DMA((17,)), pltpu.SemaphoreType.DMA((3,))],
        compiler_params=pltpu.CompilerParams(
            collective_id=1, has_side_effects=True, vmem_limit_bytes=8 * MIB
        ),
    )(st, unit)


def middle_kernel(q_ref, in_ref, g_ref, u_ref, sg, halo, pg, rows_ref, filt_ref, stat_ref, pad):
    x, y, z, c = place()
    n = z * 2 + c
    lf, lb = pg[36:37, :], pg[37:38, :]
    enter_f, enter_b = jnp.zeros((128, 128), F32), jnp.zeros((128, 128), F32)
    for j in range(16):
        state = sg[j].astype(F32)
        ahead, behind = n - 1 - j, j - n - 1
        wf = jnp.exp(lf * (ROWS * jnp.maximum(ahead, 0)).astype(F32))
        wb = jnp.exp(lb * (ROWS * jnp.maximum(behind, 0)).astype(F32))
        enter_f = enter_f + jnp.where(ahead >= 0, wf, 0.0) * state
        enter_b = enter_b + jnp.where(behind >= 0, wb, 0.0) * state
    place_ = lax.broadcasted_iota(jnp.int32, (ROWS, 128), 0).astype(F32)
    wide = q_ref[...].astype(F32)
    retained = in_ref[...]
    retained = retained + dot((wide * jnp.exp(lf * (place_ + 1.0))).astype(BF), enter_f.astype(BF))
    retained = retained + dot((wide * jnp.exp(lb * (ROWS - place_))).astype(BF), enter_b.astype(BF))
    mean = jnp.mean(retained, axis=-1, keepdims=True)
    centered = retained - mean
    variance = jnp.mean(centered * centered, axis=-1, keepdims=True)
    scaled = centered * lax.rsqrt(variance + EPS) * pg[34:35, :] + pg[35:36, :]
    rows_ref[...] = (jax.nn.silu(g_ref[...].astype(F32)) * scaled).astype(BF)

    pad[0:16, :] = jnp.where(n > 0, halo[0].astype(F32), 0.0)
    pad[16 : 16 + ROWS, :] = u_ref[...].astype(F32)
    pad[16 + ROWS :, :] = jnp.where(n < 15, halo[1].astype(F32), 0.0)
    lane = lax.broadcasted_iota(jnp.int32, (128, 128), 1)
    for i in range(ROWS // 128):
        filtered = jnp.broadcast_to(pg[31:32, :], (128, 128))
        for t in range(KERNEL):
            filtered = filtered + pg[t : t + 1, :] * pad[i * 128 + t + 1 : i * 128 + t + 129, :]
        filt_ref[i * 128 : i * 128 + 128, :] = filtered
        total = jnp.sum(filtered, axis=1, keepdims=True)
        square = jnp.sum(filtered * filtered, axis=1, keepdims=True)
        tile = jnp.where(lane == 0, total, jnp.where(lane == 1, square, 0.0))
        stat_ref[:, i * 128 : i * 128 + 128] = tile.T[0:8, :]


def middle(queries, inner, gates, unit, sg, halo, pg):
    return pl.pallas_call(
        middle_kernel,
        name="middle",
        out_shape=(
            jax.ShapeDtypeStruct((ROWS, 128), BF),
            jax.ShapeDtypeStruct((ROWS, 128), F32),
            jax.ShapeDtypeStruct((8, ROWS), F32),
        ),
        in_specs=[VM] * 7,
        out_specs=(VM,) * 3,
        scratch_shapes=[pltpu.VMEM((ROWS + 32, 128), F32)],
        compiler_params=pltpu.CompilerParams(vmem_limit_bytes=16 * MIB),
    )(queries, inner, gates, unit, sg, halo, pg)


def stats_kernel(st, all_, ss, rs):
    x, y, z, c = place()
    me = x * 4 + y
    post = Post(ss, rs)
    peers = [at((x + i) % 4, (y + j) % 4, z, c) for i in range(4) for j in range(4) if i or j]
    greet(peers)
    for peer in peers:
        post.send("s", st, all_.at[me], peer)
    all_[pl.ds(me, 1)] = st[...][None]
    post.recv("s", all_.at[pl.ds(0, 15)])
    post.finish()


def exchange_stats(st):
    return pl.pallas_call(
        stats_kernel,
        name="stats",
        out_shape=jax.ShapeDtypeStruct((16, 8, ROWS), F32),
        in_specs=[VM],
        out_specs=VM,
        scratch_shapes=[pltpu.SemaphoreType.DMA((15,)), pltpu.SemaphoreType.DMA((1,))],
        compiler_params=pltpu.CompilerParams(
            collective_id=2, has_side_effects=True, vmem_limit_bytes=8 * MIB
        ),
    )(st)


def out_kernel(rows_ref, filt_ref, stats, pg, wo, part_ref):
    total = stats[0]
    for j in range(1, 16):
        total = total + stats[j]
    for i in range(ROWS // 128):
        rows = slice(i * 128, i * 128 + 128)
        tall = jnp.concatenate([total[:, rows], jnp.zeros((120, 128), F32)], axis=0).T
        mean = tall[:, 0:1] / CONV_WIDTH
        variance = tall[:, 1:2] / CONV_WIDTH - mean * mean
        leveled = (filt_ref[rows, :] - mean) * lax.rsqrt(variance + EPS) * pg[32:33, :] + pg[33:34, :]
        both = jnp.concatenate([rows_ref[rows, :], jax.nn.silu(leveled).astype(BF)], axis=1)
        for k in range(8):
            cols = slice(k * 512, k * 512 + 512)
            part_ref[rows, cols] = dot(both, wo[:, cols]).astype(BF)


def out_part(ret_rows, filtered, stats, pg, wo):
    return pl.pallas_call(
        out_kernel,
        name="outpart",
        out_shape=jax.ShapeDtypeStruct((ROWS, 4096), BF),
        in_specs=[VM] * 5,
        out_specs=VM,
        compiler_params=pltpu.CompilerParams(vmem_limit_bytes=24 * MIB),
    )(ret_rows, filtered, stats, pg, wo)


def scatter_kernel(part, out, a2m, a2p, am, ap, ta, u, ua, b2m, b2p, bm, bp, bo, tb, v, vb, ss, rs):
    x, y, z, c = place()
    xp, xm, x2 = (x + 1) % 4, (x + 3) % 4, (x + 2) % 4
    yp, ym, y2 = (y + 1) % 4, (y + 3) % 4, (y + 2) % 4
    post = Post(ss, rs)
    partner = at(x, y, z, 1 - c)
    greet(
        [at(q, y, z, c) for q in (xp, xm, x2)]
        + [at(x, q, z, k) for q in (yp, ym, y2) for k in (0, 1)]
        + [partner]
    )
    left, right = pl.ds(0, 2048), pl.ds(2048, 2048)
    own, other = y // 2 == c, y // 2 != c
    c1p, c1m, c2 = yp // 2 == c, ym // 2 == c, y2 // 2 == c
    to_xp, to_xm = at(xp, y, z, c), at(xm, y, z, c)

    def pa(k, q):
        return part.at[k, q, :, :, left]

    def pb(yy, q0, k):
        return part.at[yy % 2, pl.ds(q0, 2), k, :, right]

    post.send("a2m", pa(0, x2), a2m, to_xp)
    post.send("a2p", pa(1, x2), a2p, to_xm)
    for k in (0, 1):
        post.send("b2m", pb(y2, 0, k), b2m.at[k], at(x, yp, z, c), c2)
        post.send("b2p", pb(y2, 2, k), b2p.at[k], at(x, ym, z, c), c2)
    post.send("am1", pa(1, xp), am.at[1], to_xp)
    post.send("ap0", pa(0, xm), ap.at[0], to_xm)
    for k in (0, 1):
        post.send("bm1", pb(yp, 2, k), bm.at[pl.ds(2, 2)], at(x, yp, z, k), c1p)
        post.send("bp0", pb(ym, 0, k), bp.at[pl.ds(0, 2)], at(x, ym, z, k), c1m)
    post.send("bo", part.at[y % 2, :, 1 - c, :, right], bo, partner, own)

    def add(a, b):
        return (a.astype(F32) + b.astype(F32)).astype(BF)

    post.recv("a2m", a2m)
    ta[0] = add(a2m[...], part[0, xp, :, :, 0:2048])
    post.send("am0", ta.at[0], am.at[0], to_xp)
    post.recv("a2p", a2p)
    ta[1] = add(a2p[...], part[1, xm, :, :, 0:2048])
    post.send("ap1", ta.at[1], ap.at[1], to_xm)

    post.recv("b2m", b2m, c1p)

    @pl.when(c1p)
    def _():
        for k in (0, 1):
            tb[0, k] = add(b2m[k], part[yp % 2, 0:2, k, :, 2048:4096])

    for k in (0, 1):
        post.send("bm0", tb.at[0, k], bm.at[pl.ds(0, 2)], at(x, yp, z, k), c1p)
    post.recv("b2p", b2p, c1m)

    @pl.when(c1m)
    def _():
        for k in (0, 1):
            tb[1, k] = add(b2p[k], part[ym % 2, 2:4, k, :, 2048:4096])

    for k in (0, 1):
        post.send("bp1", tb.at[1, k], bp.at[pl.ds(2, 2)], at(x, ym, z, k), c1m)

    @pl.when(own)
    def _():
        bo[...] = part[y % 2, :, c, :, 2048:4096]

    post.recv("am1", am.at[1])
    post.recv("ap0", ap.at[0])
    post.recv("am0", am.at[0])
    post.recv("ap1", ap.at[1])
    for k in (0, 1):
        u[k] = (part[k, x, :, :, 0:2048].astype(F32) + am[k].astype(F32) + ap[k].astype(F32)).astype(BF)
    for k in (0, 1):
        for k2 in (0, 1):
            q = 2 * c + k
            here = (q == y) & (k2 == c)
            post.send("ua", u.at[k, k2], ua.at[y], at(x, q, z, k2), jnp.logical_not(here))
            post.local("ua", u.at[k, k2], ua.at[y], here)
    post.recv("bm1", bm.at[pl.ds(2, 2)])
    post.recv("bp0", bp.at[pl.ds(0, 2)])
    post.recv("bo", bo, other)
    post.recv("bm0", bm.at[pl.ds(0, 2)])
    post.recv("bp1", bp.at[pl.ds(2, 2)])
    for q in range(4):
        v[q] = (bm[q].astype(F32) + bp[q].astype(F32) + bo[q].astype(F32)).astype(BF)
    for d, q in (("2", x2), ("p", xp), ("m", xm)):
        post.send("vb", v.at[q], vb.at[x], at(q, y, z, c))
    post.recv("ua", ua)
    out[:, 0:2048] = (
        ua[0].astype(F32) + ua[1].astype(F32) + ua[2].astype(F32) + ua[3].astype(F32)
    ).astype(BF)
    vb[pl.ds(x, 1)] = v[pl.ds(x, 1)]
    post.recv("vb", vb.at[pl.ds(0, 3)])
    out[:, 2048:4096] = (
        vb[0].astype(F32) + vb[1].astype(F32) + vb[2].astype(F32) + vb[3].astype(F32)
    ).astype(BF)
    post.finish()


def scatter(part):
    buf = lambda *shape: pltpu.VMEM((*shape, 2048), BF)
    return pl.pallas_call(
        scatter_kernel,
        name="scatter",
        out_shape=jax.ShapeDtypeStruct((32, 4096), BF),
        in_specs=[VM],
        out_specs=VM,
        scratch_shapes=[
            buf(2, 32),
            buf(2, 32),
            buf(2, 2, 32),
            buf(2, 2, 32),
            buf(2, 2, 32),
            buf(2, 2, 32),
            buf(4, 32),
            buf(2, 2, 32),
            buf(2, 2, 32),
            buf(4, 32),
            buf(4, 32),
            buf(4, 32),
            buf(2, 2, 2, 32),
            buf(4, 32),
            buf(4, 32),
            pltpu.SemaphoreType.DMA((32,)),
            pltpu.SemaphoreType.DMA((16,)),
        ],
        compiler_params=pltpu.CompilerParams(
            collective_id=3, has_side_effects=True, vmem_limit_bytes=24 * MIB
        ),
    )(part.reshape(2, 4, 2, 32, 4096))


def shards(
    hidden_states,
    norm_gain,
    query_weight,
    key_weight,
    value_weight,
    output_gate_weight,
    unit_input_weight,
    unit_gate_weight,
    decay_forward,
    decay_backward,
    group_gain,
    group_bias,
    depth_kernel,
    depth_bias,
    channel_gain,
    channel_bias,
    retention_out_weight,
    convolution_out_weight,
):
    x, y, z, c = place()
    spread = lambda decay: jnp.repeat(jax.nn.log_sigmoid(decay), HEAD_DIM)
    par = jnp.concatenate(
        [
            depth_kernel,
            jnp.stack(
                [
                    depth_bias,
                    channel_gain,
                    channel_bias,
                    group_gain,
                    group_bias,
                    spread(decay_forward),
                    spread(decay_backward),
                ]
            ),
            jnp.zeros((2, 256), F32),
        ]
    )
    half = HEAD_DIM // 2
    positions = (z * 2 + c) * ROWS + jnp.arange(ROWS, dtype=jnp.int32)
    inverse = THETA ** (-jnp.arange(half, dtype=F32) / half)
    angles = positions.astype(F32)[:, None] * inverse[None, :]
    cosine, sine = jnp.cos(angles), jnp.sin(angles)
    cosine = jnp.concatenate([cosine, cosine], axis=1)
    sine = jnp.concatenate([-sine, sine], axis=1)

    xg, wt, wo, pg = gather(
        hidden_states,
        (query_weight, key_weight, value_weight, output_gate_weight, unit_input_weight, unit_gate_weight),
        (retention_out_weight, convolution_out_weight),
        par,
    )
    queries, inner, gates, unit, st = project(xg, wt, pg, norm_gain[None, :], cosine, sine)
    sg, halo = exchange_states(st, unit)
    ret_rows, filtered, stat = middle(queries, inner, gates, unit, sg, halo, pg)
    stats = exchange_stats(stat)
    return scatter(out_part(ret_rows, filtered, stats, pg, wo))


def solution(mesh):
    split = P("sp", "tp")
    placed = (
        (split, P())
        + (split,) * 6
        + (P("tp"),) * 4
        + (P(None, "tp"),)
        + (P("tp"),) * 3
        + (P("tp", "sp"),) * 2
    )
    return jax.shard_map(
        shards, mesh=mesh, in_specs=placed, out_specs=P(("sp", "tp"), None), check_vma=False
    )
```

time: 368 us -> 151 us (0.41)
  waiting for transfers between devices: 223 us -> 0 us
  Pallas kernels: 0 us -> 136 us
  blocking collectives: 33.7 us -> 0 us
  matrix products: 31.8 us -> 0 us
  other arithmetic: 26.8 us -> 2.55 us
  starting transfers between devices: 16.5 us -> 0 us
  between operations: 13.6 us -> 0.1 us
  local copies, waits for them, and re-layouts: 20.8 us -> 11.4 us
    all_gather x3 -> x0, waiting for transfers between devices: 198 us -> none  [sent_together(): result = lax.all_gather(both, axis, axis=dim, tiled=True)]
    pallas_call x0 -> x7, Pallas kernels: none -> 136 us  [the longest x1 69.5 us: gather(): pl.pallas_call(gather_kernel, name='gather', out_shape=(jax.ShapeDtypeStr...]
    all_to_all x1 -> x0, blocking collectives: 33.7 us -> none  [sum_at_owner(): lax.all_to_all(blocks, axis, split_axis=0, concat_axis=0, tiled=True)]
    dot_general x15 -> x0, matrix products: 31.8 us -> none  [the longest x5 12.9 us: shards(): jnp.dot(normed, slab, preferred_element_type=jnp.float32)]
    all_to_all x2 -> x0, waiting for transfers between devices: 24.8 us -> none  [from_everyone(): lax.all_to_all(jnp.broadcast_to(array[None], (count, *array.shape)), axis...]
    all_to_all x2 -> x0, starting transfers between devices: 12.8 us -> none  [from_everyone(): lax.all_to_all(jnp.broadcast_to(array[None], (count, *array.shape)), axis...]
    reduce_sum x5 -> x0, other arithmetic: 7.98 us -> none  [the longest x1 6.27 us: shards(): jnp.sum(filtered, axis=1)]
    slice x5 -> x0, local copies, waits for them, and re-layouts: 3.98 us -> none  [the longest x2 3.29 us: shards(): depth_kernel[offset][None, :]]
  transfers between devices with their start and end apart: 7 -> 0, of which waited for: 5 -> 0; matrix products, arithmetic and copies ran while one was open for 11% -> 0% of each run, Pallas kernels for 0% -> 0%
where the time goes in v1:
time: 151 us; the launch traced here: 150 us
  Pallas kernels  136 us (90%)
  local copies, waits for them, and re-layouts  11.4 us (8%)
  other arithmetic  2.55 us (2%)
    pallas_call x1, Pallas kernels, gather(): pl.pallas_call(gather_kernel, name='gather', out_shape=(jax.ShapeDtypeStr...  69.5 us
    pallas_call x1, Pallas kernels, scatter(): pl.pallas_call(scatter_kernel, name='scatter', out_shape=jax.ShapeDtypeSt...  31.8 us
    pallas_call x1, Pallas kernels, exchange_states(): pl.pallas_call(states_kernel, name='states', out_shape=(jax.ShapeDtypeStr...  17.1 us
    unnamed x21, local copies, waits for them, and re-layouts  9.07 us
    pallas_call x1, Pallas kernels, exchange_stats(): pl.pallas_call(stats_kernel, name='stats', out_shape=jax.ShapeDtypeStruct...  8.44 us
    pallas_call x1, Pallas kernels, project(): pl.pallas_call(project_kernel, name='project', out_shape=(small, jax.Shap...  6.51 us

profile of v1, /device:TPU:1, one launch (start us, length us, event | category | flops | bytes accessed | tf_op | source)
XLA Modules:
  0.0 150.2 jit_solution(15284730353347879611)
XLA Ops:
  0.0 0.7 fusion.1
  0.7 0.1 broadcast_in_dim.14
  0.7 0.7 fusion.2
  1.4 0.1 broadcast_in_dim.15
  1.5 2.2 %concatenate.9.par = f32[40,256]{1,0:T(8,128)S(1)} concatenate(f32[31,256]{1,0:T(8,128)} %param.30, f32[1,256]{1,0:T(1,128)} %bitcast.11, f32[1,256]{1,0:T(1,128)} %bitcast.12, f32[1,256]{1,0:T(1,128)} %bitcast.13, f32[1,256]{1,0:T(1,128)} %bitcast.14, f32[1,256]{1,0:T(1,128)} %bitcast.15, f32[1,256]{1,0:T(1,128)S(1)} %bitcast.16, f32[1,256]{1,0:T(1,128)S(1)} %bitcast.17, ...), dimensions={0} | concatenate | bytes 81920 | tf_op jit(solution)/shard_map/concatenate | solution.py:651
  3.7 1.0 fusion
  4.7 0.2 pad_maximum_fusion
  4.9 0.0 copy-start
  4.9 0.9 copy-done
  5.9 0.0 copy-start.1
  5.9 0.8 copy-done.1
  6.7 0.0 copy-start.2
  6.7 0.8 copy-done.2
  7.6 0.0 copy-start.3
  7.6 0.8 copy-done.3
  8.4 0.0 copy-start.4
  8.4 0.8 copy-done.4
  9.2 0.0 copy-start.5
  9.2 0.8 copy-done.5
  10.1 0.0 copy-start.6
  10.1 0.8 copy-done.6
  10.9 0.0 copy-start.7
  10.9 0.8 copy-done.7
  11.8 0.0 copy-start.8
  11.8 0.8 copy-done.8
  12.6 69.5 %gather.1 = (bf16[512,4096]{1,0:T(8,128)(2,1)S(1)}, bf16[4096,768]{1,0:T(8,128)(2,1)S(1)}, bf16[256,4096]{1,0:T(8,128)(2,1)S(1)}, f32[40,128]{1,0:T(8,128)S(1)}) custom-call(bf16[256,512]{1,0:T(8,128)(2,1)S(1)} %copy-done, bf16[128,256]{1,0:T(8,128)(2,1)S(1)} %copy-done.1, bf16[128,256]{1,0:T(8,128)(2,1)S(1)} %copy-done.2, bf16[128,256]{1,0:T(8,128)(2,1)S(1)} %copy-done.3, ...), custom_call_target="tpu_custom_call" | custom-call | tf_op jit(solution)/shard_map/gather/pallas_call | solution.py:268
  82.1 0.0 copy-start.9
  82.1 0.7 copy-done.9
  82.8 6.5 %project.1 = (bf16[512,128]{1,0:T(8,128)(2,1)S(1)}, f32[512,128]{1,0:T(8,128)S(1)}, bf16[512,128]{1,0:T(8,128)(2,1)S(1)}, bf16[512,128]{1,0:T(8,128)(2,1)S(1)}, bf16[2,128,128]{2,1,0:T(8,128)(2,1)S(1)}) custom-call(bf16[512,4096]{1,0:T(8,128)(2,1)S(1)} %get-tuple-element.19.xg, bf16[4096,768]{1,0:T(8,128)(2,1)S(1)} %get-tuple-element.20.wt, ...), custom_call_target="tpu_custom_call" | custom-call | tf_op jit(solution)/shard_map/project/pallas_call | solution.py:334
  89.3 17.1 %states.1 = (bf16[16,128,128]{2,1,0:T(8,128)(2,1)S(1)}, bf16[2,16,128]{2,1,0:T(8,128)(2,1)S(1)}) custom-call(bf16[2,128,128]{2,1,0:T(8,128)(2,1)S(1)} %get-tuple-element.26.st, bf16[512,128]{1,0:T(8,128)(2,1)S(1)} %get-tuple-element.25.unit.u_ref), custom_call_target="tpu_custom_call" | custom-call | tf_op jit(solution)/shard_map/states/pallas_call | solution.py:375
  106.4 1.5 middle.1
  107.8 8.4 %stats.1 = f32[16,8,512]{2,1,0:T(8,128)S(1)} custom-call(f32[8,512]{1,0:T(8,128)S(1)} %get-tuple-element.31.st), custom_call_target="tpu_custom_call" | custom-call | tf_op jit(solution)/shard_map/stats/pallas_call | solution.py:456
  116.3 1.5 outpart.1
  117.8 31.8 %scatter.1 = bf16[32,4096]{1,0:T(8,128)(2,1)S(1)} custom-call(bf16[2,4,2,32,4096]{4,3,2,1,0:T(8,128)(2,1)S(1)} %bitcast.9), custom_call_target="tpu_custom_call" | custom-call | tf_op jit(solution)/shard_map/scatter/pallas_call | solution.py:598
  149.5 0.7 copy.20
  (3 shorter events, 0.0 us)
Async XLA Ops:
  4.9 1.0 copy-start
  5.9 0.8 copy-start.1
  6.7 0.8 copy-start.2
  7.6 0.8 copy-start.3
  8.4 0.8 copy-start.4
  9.2 0.8 copy-start.5
  10.1 0.8 copy-start.6
  10.9 0.8 copy-start.7
  11.8 0.8 copy-start.8
  82.1 0.7 copy-start.9

commit v2 on v1

v2 whole, which is shorter than its diff:
```python
import functools

import jax
import jax.numpy as jnp
import numpy as np
from jax import lax
from jax.experimental import pallas as pl
from jax.experimental.pallas import tpu as pltpu
from jax.sharding import PartitionSpec as P

HEAD_DIM = 128
CONV_WIDTH = 2048
KERNEL = 31
EPS = 1e-06
THETA = 10000.0
ROWS = 512
BF = jnp.bfloat16
F32 = jnp.float32
MESH = pl.DeviceIdType.MESH
VM = pl.BlockSpec(memory_space=pltpu.VMEM)
HBM = pl.BlockSpec(memory_space=pltpu.HBM)
SM = pl.BlockSpec(memory_space=pltpu.SMEM)
MIB = 1 << 20


def place():
    sp, tp = lax.axis_index("sp"), lax.axis_index("tp")
    return tp // 2, sp % 4, sp // 4, tp % 2


def at(x, y, z, c):
    return (z * 4 + y, x * 2 + c)


def when(cond, f):
    if cond is None:
        f()
    else:
        pl.when(cond)(f)


class Post:
    def __init__(self, send_sems, recv_sems):
        self.ss, self.rs = send_sems, recv_sems
        self.sent, self.ids = [], {}

    def key(self, name):
        return self.rs.at[self.ids.setdefault(name, len(self.ids))]

    def send(self, name, src, dst, to, cond=None, recv=None):
        sem = self.ss.at[len(self.sent)]
        recv = self.key(name) if recv is None else recv

        def make():
            return pltpu.make_async_remote_copy(
                src_ref=src, dst_ref=dst, send_sem=sem, recv_sem=recv, device_id=to, device_id_type=MESH
            )

        self.sent.append((make, cond))
        when(cond, lambda: make().start())

    def local(self, name, src, dst, cond=None, recv=None):
        recv = self.key(name) if recv is None else recv
        when(cond, lambda: pltpu.make_async_copy(src, dst, recv).start())

    def recv(self, name, ref, cond=None, recv=None):
        recv = self.key(name) if recv is None else recv
        when(cond, lambda: pltpu.make_async_copy(ref, ref, recv).wait())

    def finish(self):
        for make, cond in self.sent:
            when(cond, lambda: make().wait_send())


def greet(peers):
    barrier = pltpu.get_barrier_semaphore()
    for peer in peers:
        pl.semaphore_signal(barrier, inc=1, device_id=peer, device_id_type=MESH)
    pl.semaphore_wait(barrier, len(peers))


def rows_at(start, size, unit=16):
    return pl.ds(pl.multiple_of(start, unit), size)


def cols_at(start, size):
    return pl.ds(pl.multiple_of(start, 128), size)


def dot(a, b, dims=((1,), (0,))):
    return lax.dot_general(a, b, (dims, ((), ())), preferred_element_type=F32)


def log_sigmoid(decay):
    t = jnp.exp(-decay)
    s = t / (2.0 + t)
    square = s * s
    series = jnp.full_like(s, 1.0 / 15)
    for n in (13, 11, 9, 7, 5, 3, 1):
        series = series * square + 1.0 / n
    return -2.0 * s * series


def mixer_kernel(
    xin, wq, wk, wv, wg, wa, wb, wr, wc, dk_in, pv_in, gain_in, cos_in, sin_in, base_in, df, db, out,
    xg, nrm, wt, wo, dk, pv, gain, cosine, sine, base, dec, decp, qs, inner, gs, us, st, sg, halo,
    pad, filt, stat, stats, both, part,
    a2m, a2p, am, ap, ta, u, ua, b2m, b2p, bm, bp, bo, tb, v, vb, ss, rs,
):
    x, y, z, c = place()
    n = z * 2 + c
    ct, yl = y // 2, y % 2
    xp, xm, x2 = (x + 1) % 4, (x + 3) % 4, (x + 2) % 4
    yp, ym, y2 = (y + 1) % 4, (y + 3) % 4, (y + 2) % 4
    zp, zm = (z + 1) % 8, (z + 7) % 8
    own = ct == c
    other = ct != c
    post = Post(ss, rs)
    partner = at(x, y, z, 1 - c)
    post.local("gain", gain_in, gain)
    post.local("cos", cos_in, cosine)
    post.local("sin", sin_in, sine)
    post.local("base", base_in, base)
    line = [(dz, (z + dz) % 8) for dz in range(1, 8)]
    greet(
        [at(x, y, q, k) for _, q in line for k in (0, 1)]
        + [partner]
        + [at((x + i) % 4, (y + j) % 4, z, c) for i in range(4) for j in range(4) if i or j]
        + [at(q, y, z, 1 - c) for q in (xp, xm)]
        + [at(x, q, z, 1 - c) for q in (yp, ym, y2)]
    )

    def xblock(yy, half, r0, rn, col, width):
        return xg.at[rows_at((yy % 2) * 256 + half * 128 + r0, rn), cols_at(col, width)]

    s = z * 4 + y
    post.key("w0"), post.key("w1")
    wsem = rs.at[post.ids["w0"] + yl]
    for j in (0, 1):
        q = 2 * c + j
        here = (q == y) & own
        away = jnp.logical_not(here)
        to = at(x, q, z, ct)
        for m, w in enumerate((wq, wk, wv, wg, wa, wb)):
            src, dst = w.at[:, pl.ds(j * 128, 128)], wt.at[rows_at(s * 128, 128), pl.ds(m * 128, 128)]
            post.local("w", src, dst, here, wsem)
            post.send("w", src, dst, to, away, wsem)

    mine = (x * 2 + c) * 512
    for half, name, ends in ((0, "x1", ((xp, y, "m"), (xm, y, "p"))), (1, "x2", ((x, yp, "m"), (x, ym, "p")))):
        src, dst = xin.at[pl.ds(half * 128, 128), :], xblock(y, half, 0, 128, mine, 512)
        for qx, qy, d in ends:
            post.send(name + d, src, dst, at(qx, qy, z, ct))
        post.send(name + "l", src, dst, partner, other)
        post.local(name + "s", src, dst, own)

    for j in (0, 1):
        q = 2 * c + j
        here = (q == y) & own
        away = jnp.logical_not(here)
        to = at(x, q, z, ct)
        for m, w in enumerate((wr, wc)):
            src, dst = w.at[pl.ds(j * 128, 128), :], wo.at[pl.ds(m * 128, 128), cols_at(s * 128, 128)]
            post.send("o", src, dst, to, away)
            post.local("o", src, dst, here)
    for name, ref, dst in (("dk", dk_in, dk), ("pv", pv_in, pv)):
        src = ref.at[:, cols_at(yl * 128, 128)]
        post.send(name, src, dst, partner, own)
        post.local(name, src, dst, own)
    decp[0:1, :] = log_sigmoid(jnp.full((1, 128), df[yl], F32))
    decp[1:2, :] = log_sigmoid(jnp.full((1, 128), db[yl], F32))

    def wrows(zz, i, r0=0, rn=128):
        sub = yl if i == 0 else 1 - yl
        return wt.at[rows_at((zz * 4 + 2 * c + sub) * 128 + r0, rn), :]

    def zsend(zz, i, r, d, r0=0, rn=128):
        ref = wrows(zz, i, r0, rn)
        post.send(("z", d, r, i), ref, ref, at(x, y, zp if d == "m" else zm, c))

    def zpass(zz, i, rel, r0=0, rn=128):
        ref = wrows(zz, i, r0, rn)
        post.send(("zp", rel, i, r0), ref, ref, partner)

    def ocols(zz, core=c, r0=0, rn=256):
        return wo.at[pl.ds(r0, rn), cols_at((zz * 4 + 2 * core) * 128, 256)]

    def osend(zz, r, d, r0=0, rn=256):
        ref = ocols(zz, c, r0, rn)
        post.send(("o", d, r), ref, ref, at(x, y, zp if d == "m" else zm, c))

    def opass(zz, rel, r0=0, rn=256):
        ref = ocols(zz, c, r0, rn)
        post.send(("op", rel, r0), ref, ref, partner)

    for i in (0, 1):
        post.recv("w", wrows(z, i), None, rs.at[post.ids["w0"] + (yl if i == 0 else 1 - yl)])
        for d in ("m", "p"):
            zsend(z, i, 1, d)
        zpass(z, i, 0)
    post.send("dec", decp, dec, partner, own)

    cm, cp, c2 = ym // 2 == c, yp // 2 == c, y2 // 2 == c
    post.recv("x1m", xblock(y, 0, 0, 128, xm * 1024, 1024), own)
    ref = xblock(y, 0, 0, 64, xm * 1024, 1024)
    post.send("x1m2", ref, ref, at(xp, y, z, c), own)
    post.recv("x1p", xblock(y, 0, 0, 128, xp * 1024, 1024), own)
    ref = xblock(y, 0, 64, 64, xp * 1024, 1024)
    post.send("x1p2", ref, ref, at(xm, y, z, c), own)
    post.recv("x2m", xblock(ym, 1, 0, 128, x * 1024, 1024), cm)
    ref = xblock(ym, 1, 0, 64, x * 1024, 1024)
    post.send("x2m2", ref, ref, at(x, yp, z, c), cm)
    post.recv("x2p", xblock(yp, 1, 0, 128, x * 1024, 1024), cp)
    ref = xblock(yp, 1, 64, 64, x * 1024, 1024)
    post.send("x2p2", ref, ref, at(x, ym, z, c), cp)

    for name, half in (("x1", 0), ("x2", 1)):
        block = xblock(y, half, 0, 128, mine, 512)
        post.recv(name + "s", block, own)
        post.recv(name + "l", xblock(y, half, 0, 128, (x * 2 + 1 - c) * 512, 512), own)
    post.recv("x1m2", xblock(y, 0, 0, 64, x2 * 1024, 1024), own)
    post.recv("x1p2", xblock(y, 0, 64, 64, x2 * 1024, 1024), own)
    for i in (0, 1):
        ref = xblock(y, 0, i * 64, 64, 0, 4096)
        post.send(("x3m", i), ref, ref, at(x, yp, z, c), own)
    for i in (1, 0):
        ref = xblock(y, 0, i * 64, 64, 0, 4096)
        post.send(("x3p", i), ref, ref, at(x, ym, z, c), own)
    post.recv("x2m2", xblock(y2, 1, 0, 64, x * 1024, 1024), c2)
    post.recv("x2p2", xblock(y2, 1, 64, 64, x * 1024, 1024), c2)

    def x4(qx, k):
        return xblock(k, 1, 0, 128, qx * 1024, 1024)

    for d, to, order in (("m", xp, (0, 1)), ("p", xm, (1, 0))):
        for k in order:
            post.send(("x4" + d, k), x4(x, k), x4(x, k), at(to, y, z, c))

    def zstep(r):
        for i in (0, 1):
            for d in ("m", "p"):
                zz = (z - r) % 8 if d == "m" else (z + r) % 8
                post.recv(("z", d, r, i), wrows(zz, i))
                if r < 3:
                    zsend(zz, i, r + 1, d)
                else:
                    zsend(zz, i, 4, d, 0 if d == "m" else 64, 64)
                zpass(zz, i, -r % 8 if d == "m" else r)

    def ostep(r):
        for d in ("m", "p"):
            zz = (z - r) % 8 if d == "m" else (z + r) % 8
            post.recv(("o", d, r), ocols(zz))
            if r < 3:
                osend(zz, r + 1, d)
            else:
                osend(zz, 4, d, 0 if d == "m" else 128, 128)
            opass(zz, -r % 8 if d == "m" else r)

    zstep(1)
    post.recv(("x3m", 0), xblock(ym, 0, 0, 64, 0, 4096), cm)
    ref = xblock(ym, 0, 0, 64, 0, 4096)
    post.send("x3m2", ref, ref, at(x, yp, z, c), cm)
    post.recv(("x3p", 1), xblock(yp, 0, 64, 64, 0, 4096), cp)
    ref = xblock(yp, 0, 64, 64, 0, 4096)
    post.send("x3p2", ref, ref, at(x, ym, z, c), cp)
    post.recv(("x4m", 0), x4(xm, 0))
    post.send("x4m2", x4(xm, 0), x4(xm, 0), at(xp, y, z, c))
    post.recv(("x4p", 1), x4(xp, 1))
    post.send("x4p2", x4(xp, 1), x4(xp, 1), at(xm, y, z, c))
    zstep(2)
    post.recv("o", ocols(z))
    zstep(3)
    for d in ("m", "p"):
        osend(z, 1, d)
    opass(z, 0)
    post.recv(("x3m", 1), xblock(ym, 0, 64, 64, 0, 4096), cm)
    post.recv(("x3p", 0), xblock(yp, 0, 0, 64, 0, 4096), cp)
    post.recv("x3m2", xblock(y2, 0, 0, 64, 0, 4096), c2)
    post.recv("x3p2", xblock(y2, 0, 64, 64, 0, 4096), c2)
    post.recv(("x4m", 1), x4(xm, 1))
    post.recv(("x4p", 0), x4(xp, 0))
    post.recv("x4m2", x4(x2, 0))
    post.recv("x4p2", x4(x2, 1))
    for name, ref in (("gain", gain), ("cos", cosine), ("sin", sine), ("base", base), ("dk", dk), ("pv", pv)):
        post.recv(name, ref)

    @pl.loop(0, ROWS // 128)
    def _(i):
        rows = rows_at(i * 128, 128)
        square = jnp.zeros((128, 128), F32)
        for k in range(32):
            piece = xg[rows, k * 128 : k * 128 + 128].astype(F32)
            square = square + piece * piece
        scale = lax.rsqrt(jnp.sum(square, axis=1, keepdims=True) / 4096 + EPS)
        for k in range(32):
            cols = slice(k * 128, k * 128 + 128)
            nrm[rows, cols] = (xg[rows, cols].astype(F32) * scale * gain[:, cols]).astype(BF)

    far = (z + 4) % 8
    for i in (0, 1):
        for d, r0 in (("m", 0), ("p", 64)):
            post.recv(("z", d, 4, i), wrows(far, i, r0, 64))
            zpass(far, i, 4, r0, 64)
    ostep(1)
    post.recv("dec", dec, other)

    @pl.when(own)
    def _():
        dec[...] = decp[...]

    for rel in range(8):
        zz = (z + rel) % 8
        for i in (0, 1):
            sub = yl if i == 0 else 1 - yl
            for r0, rn in ((0, 64), (64, 64)) if rel == 4 else ((0, 128),):
                row = (zz * 4 + 2 * (1 - c) + sub) * 128 + r0
                post.recv(("zp", rel, i, r0), wt.at[rows_at(row, rn), :])

    proj = dot(nrm[...], wt[...]).astype(BF)
    cb, sb = base[n][:, 0:128], base[n][:, 128:256]
    cosine[...], sine[...] = cosine[...] * cb - sine[...] * sb, sine[...] * cb + cosine[...] * sb

    def turn(rows):
        wide = rows.astype(F32)
        return (wide * cosine[...] + pltpu.roll(wide, 64, axis=1) * sine[...]).astype(BF)

    keys, values = turn(proj[:, 128:256]), proj[:, 256:384]
    us[...] = (proj[:, 512:640].astype(F32) * jax.nn.sigmoid(proj[:, 640:768].astype(F32))).astype(BF)
    after, before = (n + 1) % 16, (n + 15) % 16
    post.send("ht", us.at[pl.ds(ROWS - 16, 16), :], halo.at[0], at(x, y, after // 2, after % 2))
    post.send("hh", us.at[pl.ds(0, 16), :], halo.at[1], at(x, y, before // 2, before % 2))
    lf, lb = dec[0:1, :], dec[1:2, :]
    place_ = lax.broadcasted_iota(jnp.int32, (ROWS, 128), 0).astype(F32)
    wide = keys.astype(F32)
    st[0] = dot((wide * jnp.exp(lb * place_)).astype(BF), values, ((0,), (0,))).astype(BF)
    st[1] = dot((wide * jnp.exp(lf * (ROWS - 1.0 - place_))).astype(BF), values, ((0,), (0,))).astype(BF)
    for dz, q in line:
        post.send(("st", dz), st.at[(q * 2 - z * 2 + 16) // 16], sg.at[n], at(x, y, q, c))
    post.send("sp", st.at[1 - c], sg.at[n], partner)
    queries = turn(proj[:, 0:128])
    gs[...] = proj[:, 384:512]
    qs[...] = queries
    f1, b1 = lf[:, 0:1], lb[:, 0:1]
    for i in range(ROWS // 128):
        rows = slice(i * 128, i * 128 + 128)
        gap = (
            lax.broadcasted_iota(jnp.int32, (128, ROWS), 0)
            + i * 128
            - lax.broadcasted_iota(jnp.int32, (128, ROWS), 1)
        ).astype(F32)
        decay = jnp.exp(jnp.where(gap >= 0, f1 * gap, -b1 * gap))
        scores = dot(queries[rows], keys, ((1,), (1,))) * decay
        inner[rows, :] = dot(scores.astype(BF), values)
    ostep(2)

    post.recv("ht", halo.at[0])
    post.recv("hh", halo.at[1])
    pad[0:16, :] = jnp.where(n > 0, halo[0].astype(F32), 0.0)
    pad[16 : 16 + ROWS, :] = us[...].astype(F32)
    pad[16 + ROWS :, :] = jnp.where(n < 15, halo[1].astype(F32), 0.0)
    lane = lax.broadcasted_iota(jnp.int32, (128, 128), 1)
    for i in range(ROWS // 128):
        filtered = jnp.broadcast_to(pv[0:1, :], (128, 128))
        for t in range(KERNEL):
            filtered = filtered + dk[t : t + 1, :] * pad[i * 128 + t + 1 : i * 128 + t + 129, :]
        filt[i * 128 : i * 128 + 128, :] = filtered
        total = jnp.sum(filtered, axis=1, keepdims=True)
        square = jnp.sum(filtered * filtered, axis=1, keepdims=True)
        tile = jnp.where(lane == 0, total, jnp.where(lane == 1, square, 0.0))
        stat[:, i * 128 : i * 128 + 128] = tile.T[0:8, :]
    me = x * 4 + y
    for i in range(4):
        for j in range(4):
            if i or j:
                post.send("stats", stat, stats.at[me], at((x + i) % 4, (y + j) % 4, z, c))
    stats[pl.ds(me, 1)] = stat[...][None]
    sg[pl.ds(n, 1)] = jnp.zeros((1, 128, 128), BF)

    for dz, q in line:
        slot = sg.at[((z - dz) % 8) * 2 + c]
        post.recv(("st", dz), slot)
        post.send(("sp", dz), slot, slot, partner)
    ostep(3)
    post.recv("sp", sg.at[z * 2 + 1 - c])
    for dz, q in line:
        post.recv(("sp", dz), sg.at[((z - dz) % 8) * 2 + 1 - c])
    enter_f, enter_b = jnp.zeros((128, 128), F32), jnp.zeros((128, 128), F32)
    for j in range(16):
        state = sg[j].astype(F32)
        ahead, behind = n - 1 - j, j - n - 1
        wf = jnp.exp(lf * (ROWS * jnp.maximum(ahead, 0)).astype(F32))
        wb_ = jnp.exp(lb * (ROWS * jnp.maximum(behind, 0)).astype(F32))
        enter_f = enter_f + jnp.where(ahead >= 0, wf, 0.0) * state
        enter_b = enter_b + jnp.where(behind >= 0, wb_, 0.0) * state
    wide = qs[...].astype(F32)
    retained = inner[...]
    retained = retained + dot((wide * jnp.exp(lf * (place_ + 1.0))).astype(BF), enter_f.astype(BF))
    retained = retained + dot((wide * jnp.exp(lb * (ROWS - place_))).astype(BF), enter_b.astype(BF))
    mean = jnp.mean(retained, axis=-1, keepdims=True)
    centered = retained - mean
    variance = jnp.mean(centered * centered, axis=-1, keepdims=True)
    scaled = centered * lax.rsqrt(variance + EPS) * pv[3:4, :] + pv[4:5, :]
    both[:, 0:128] = (jax.nn.silu(gs[...].astype(F32)) * scaled).astype(BF)

    for d, r0 in (("m", 0), ("p", 128)):
        post.recv(("o", d, 4), ocols(far, c, r0, 128))
        opass(far, 4, r0, 128)
    post.recv("stats", stats.at[pl.ds(0, 15)])
    total = stats[0]
    for j in range(1, 16):
        total = total + stats[j]
    for i in range(ROWS // 128):
        rows = slice(i * 128, i * 128 + 128)
        tall = jnp.concatenate([total[:, rows], jnp.zeros((120, 128), F32)], axis=0).T
        mean = tall[:, 0:1] / CONV_WIDTH
        variance = tall[:, 1:2] / CONV_WIDTH - mean * mean
        leveled = (filt[rows, :] - mean) * lax.rsqrt(variance + EPS) * pv[1:2, :] + pv[2:3, :]
        both[rows, 128:256] = jax.nn.silu(leveled).astype(BF)
    for rel in range(8):
        zz = (z + rel) % 8
        for r0, rn in ((0, 128), (128, 128)) if rel == 4 else ((0, 256),):
            post.recv(("op", rel, r0), ocols(zz, 1 - c, r0, rn))

    def out_part(first, last):
        for k in range(first, last):
            cols = slice(k * 512, k * 512 + 512)
            part[:, :, :, :, cols] = dot(both[...], wo[:, cols]).astype(BF).reshape(2, 4, 2, 32, 512)

    left, right = pl.ds(0, 2048), pl.ds(2048, 2048)
    to_xp, to_xm = at(xp, y, z, c), at(xm, y, z, c)
    c1p, c1m = cp, cm

    def pa(k, q):
        return part.at[k, q, :, :, left]

    def pb(yy, q0, k):
        return part.at[yy % 2, pl.ds(q0, 2), k, :, right]

    out_part(0, 4)
    post.send("a2m", pa(0, x2), a2m, to_xp)
    post.send("a2p", pa(1, x2), a2p, to_xm)
    post.send("am1", pa(1, xp), am.at[1], to_xp)
    post.send("ap0", pa(0, xm), ap.at[0], to_xm)
    out_part(4, 8)
    for k in (0, 1):
        post.send("b2m", pb(y2, 0, k), b2m.at[k], at(x, yp, z, c), c2)
        post.send("b2p", pb(y2, 2, k), b2p.at[k], at(x, ym, z, c), c2)
    for k in (0, 1):
        post.send("bm1", pb(yp, 2, k), bm.at[pl.ds(2, 2)], at(x, yp, z, k), c1p)
        post.send("bp0", pb(ym, 0, k), bp.at[pl.ds(0, 2)], at(x, ym, z, k), c1m)
    post.send("bo", part.at[y % 2, :, 1 - c, :, right], bo, partner, own)

    def add(a, b):
        return (a.astype(F32) + b.astype(F32)).astype(BF)

    post.recv("a2m", a2m)
    ta[0] = add(a2m[...], part[0, xp, :, :, 0:2048])
    post.send("am0", ta.at[0], am.at[0], to_xp)
    post.recv("a2p", a2p)
    ta[1] = add(a2p[...], part[1, xm, :, :, 0:2048])
    post.send("ap1", ta.at[1], ap.at[1], to_xm)

    post.recv("b2m", b2m, c1p)

    @pl.when(c1p)
    def _():
        for k in (0, 1):
            tb[0, k] = add(b2m[k], part[yp % 2, 0:2, k, :, 2048:4096])

    for k in (0, 1):
        post.send("bm0", tb.at[0, k], bm.at[pl.ds(0, 2)], at(x, yp, z, k), c1p)
    post.recv("b2p", b2p, c1m)

    @pl.when(c1m)
    def _():
        for k in (0, 1):
            tb[1, k] = add(b2p[k], part[ym % 2, 2:4, k, :, 2048:4096])

    for k in (0, 1):
        post.send("bp1", tb.at[1, k], bp.at[pl.ds(2, 2)], at(x, ym, z, k), c1m)

    @pl.when(own)
    def _():
        bo[...] = part[y % 2, :, c, :, 2048:4096]

    post.recv("am1", am.at[1])
    post.recv("ap0", ap.at[0])
    post.recv("am0", am.at[0])
    post.recv("ap1", ap.at[1])
    for k in (0, 1):
        u[k] = (part[k, x, :, :, 0:2048].astype(F32) + am[k].astype(F32) + ap[k].astype(F32)).astype(BF)
    for k in (0, 1):
        for k2 in (0, 1):
            q = 2 * c + k
            here = (q == y) & (k2 == c)
            post.send("ua", u.at[k, k2], ua.at[y], at(x, q, z, k2), jnp.logical_not(here))
            post.local("ua", u.at[k, k2], ua.at[y], here)
    post.recv("bm1", bm.at[pl.ds(2, 2)])
    post.recv("bp0", bp.at[pl.ds(0, 2)])
    post.recv("bo", bo, other)
    post.recv("bm0", bm.at[pl.ds(0, 2)])
    post.recv("bp1", bp.at[pl.ds(2, 2)])
    for q in range(4):
        v[q] = (bm[q].astype(F32) + bp[q].astype(F32) + bo[q].astype(F32)).astype(BF)
    for d, q in (("2", x2), ("p", xp), ("m", xm)):
        post.send("vb", v.at[q], vb.at[x], at(q, y, z, c))
    post.recv("ua", ua)
    out[:, 0:2048] = (
        ua[0].astype(F32) + ua[1].astype(F32) + ua[2].astype(F32) + ua[3].astype(F32)
    ).astype(BF)
    vb[pl.ds(x, 1)] = v[pl.ds(x, 1)]
    post.recv("vb", vb.at[pl.ds(0, 3)])
    out[:, 2048:4096] = (
        vb[0].astype(F32) + vb[1].astype(F32) + vb[2].astype(F32) + vb[3].astype(F32)
    ).astype(BF)
    post.finish()


def table():
    half = HEAD_DIM // 2
    inverse = np.tile(THETA ** (-np.arange(half) / half), 2)
    sign = np.repeat([-1.0, 1.0], half)
    near = np.arange(ROWS)[:, None] * inverse
    far = np.arange(16)[:, None] * ROWS * inverse
    base = np.concatenate([np.cos(far), sign * np.sin(far)], axis=1)
    return [a.astype(np.float32) for a in (np.cos(near), sign * np.sin(near), base[:, None])]


def shards(
    hidden_states,
    norm_gain,
    query_weight,
    key_weight,
    value_weight,
    output_gate_weight,
    unit_input_weight,
    unit_gate_weight,
    decay_forward,
    decay_backward,
    group_gain,
    group_bias,
    depth_kernel,
    depth_bias,
    channel_gain,
    channel_bias,
    retention_out_weight,
    convolution_out_weight,
):
    vectors = jnp.stack([depth_bias, channel_gain, channel_bias, group_gain, group_bias])
    buf = lambda *shape: pltpu.VMEM((*shape, 2048), BF)
    small = lambda dtype: pltpu.VMEM((ROWS, 128), dtype)
    return pl.pallas_call(
        mixer_kernel,
        name="mixer",
        out_shape=jax.ShapeDtypeStruct((32, 4096), BF),
        in_specs=[HBM] * 15 + [SM] * 2,
        out_specs=VM,
        scratch_shapes=[
            pltpu.VMEM((ROWS, 4096), BF),
            pltpu.VMEM((ROWS, 4096), BF),
            pltpu.VMEM((4096, 768), BF),
            pltpu.VMEM((256, 4096), BF),
            pltpu.VMEM((KERNEL, 128), F32),
            pltpu.VMEM((5, 128), F32),
            pltpu.VMEM((1, 4096), F32),
            small(F32),
            small(F32),
            pltpu.VMEM((16, 1, 256), F32),
            pltpu.VMEM((8, 128), F32),
            pltpu.VMEM((8, 128), F32),
            small(BF),
            small(F32),
            small(BF),
            small(BF),
            pltpu.VMEM((2, 128, 128), BF),
            pltpu.VMEM((16, 128, 128), BF),
            pltpu.VMEM((2, 16, 128), BF),
            pltpu.VMEM((ROWS + 32, 128), F32),
            small(F32),
            pltpu.VMEM((8, ROWS), F32),
            pltpu.VMEM((16, 8, ROWS), F32),
            pltpu.VMEM((ROWS, 256), BF),
            pltpu.VMEM((2, 4, 2, 32, 4096), BF),
            buf(2, 32),
            buf(2, 32),
            buf(2, 2, 32),
            buf(2, 2, 32),
            buf(2, 2, 32),
            buf(2, 2, 32),
            buf(4, 32),
            buf(2, 2, 32),
            buf(2, 2, 32),
            buf(4, 32),
            buf(4, 32),
            buf(4, 32),
            buf(2, 2, 2, 32),
            buf(4, 32),
            buf(4, 32),
            pltpu.SemaphoreType.DMA((200,)),
            pltpu.SemaphoreType.DMA((140,)),
        ],
        compiler_params=pltpu.CompilerParams(
            collective_id=0, has_side_effects=True, vmem_limit_bytes=48 * MIB
        ),
    )(
        hidden_states,
        query_weight,
        key_weight,
        value_weight,
        output_gate_weight,
        unit_input_weight,
        unit_gate_weight,
        retention_out_weight,
        convolution_out_weight,
        depth_kernel,
        vectors,
        norm_gain.reshape(1, -1),
        *table(),
        decay_forward,
        decay_backward,
    )


def solution(mesh):
    split = P("sp", "tp")
    placed = (
        (split, P())
        + (split,) * 6
        + (P("tp"),) * 4
        + (P(None, "tp"),)
        + (P("tp"),) * 3
        + (P("tp", "sp"),) * 2
    )
    return jax.shard_map(
        shards, mesh=mesh, in_specs=placed, out_specs=P(("sp", "tp"), None), check_vma=False
    )
```

time: 151 us -> 117 us (0.77)
  Pallas kernels: 136 us -> 104 us
  other arithmetic: 2.55 us -> 0 us
    pallas_call x7 -> x1, Pallas kernels: 136 us -> 104 us  [shards(): pl.pallas_call(mixer_kernel, name='mixer', out_shape=jax.ShapeDtypeStruct...]
    unnamed x21 -> x33, local copies, waits for them, and re-layouts: 9.07 us -> 11.7 us
    neg x3 -> x0, other arithmetic: 2.33 us -> none  [the longest x2 1.34 us: shards(): spread = lambda decay: jnp.repeat(jax.nn.log_sigmoid(decay), HEAD_DIM)]
    concatenate x1 -> x0, local copies, waits for them, and re-layouts: 2.21 us -> none  [shards(): jnp.concatenate([depth_kernel, jnp.stack([depth_bias, channel_gain, chann...]
where the time goes in v2:
time: 117 us; the launch traced here: 116 us
  Pallas kernels  104 us (89%)
  local copies, waits for them, and re-layouts  12.5 us (11%)
    pallas_call x1, Pallas kernels, shards(): pl.pallas_call(mixer_kernel, name='mixer', out_shape=jax.ShapeDtypeStruct...  104 us
    unnamed x33, local copies, waits for them, and re-layouts  11.7 us

profile of v2, /device:TPU:1, one launch (start us, length us, event | category | flops | bytes accessed | tf_op | source)
XLA Modules:
  0.0 116.4 jit_solution(697937655507981414)
XLA Ops:
  0.0 0.0 copy-start.12
  0.0 0.0 copy-start.14
  0.0 0.0 copy-start.15
  0.0 0.8 stack.23.pv_in
  0.8 0.0 copy-done.12
  0.8 0.0 copy-done.14
  0.8 0.0 copy-done.15
  0.8 0.0 copy-start
  0.8 0.9 copy-done
  1.8 0.0 copy-start.1
  1.8 0.9 copy-done.1
  2.7 0.0 copy-start.2
  2.7 0.9 copy-done.2
  3.7 0.0 copy-start.3
  3.7 0.8 copy-done.3
  4.5 0.0 copy-start.4
  4.5 0.8 copy-done.4
  5.4 0.0 copy-start.5
  5.4 0.8 copy-done.5
  6.2 0.0 copy-start.6
  6.2 0.8 copy-done.6
  7.0 0.0 copy-start.7
  7.1 0.8 copy-done.7
  7.9 0.0 copy-start.8
  7.9 0.8 copy-done.8
  8.7 0.0 copy-start.9
  8.7 0.8 copy-done.9
  9.6 0.0 copy-start.10
  9.6 0.8 copy-done.10
  10.4 0.0 copy-start.11
  10.4 0.8 copy-done.11
  11.2 0.0 copy-start.13
  11.2 0.7 copy-done.13
  11.9 103.8 %mixer.1 = bf16[32,4096]{1,0:T(8,128)(2,1)S(1)} custom-call(bf16[256,512]{1,0:T(8,128)(2,1)S(1)} %copy-done, bf16[128,256]{1,0:T(8,128)(2,1)S(1)} %copy-done.3, bf16[128,256]{1,0:T(8,128)(2,1)S(1)} %copy-done.4, bf16[128,256]{1,0:T(8,128)(2,1)S(1)} %copy-done.5, bf16[128,256]{1,0:T(8,128)(2,1)S(1)} %copy-done.6, bf16[128,256]{1,0:T(8,128)(2,1)S(1)} %copy-done.7, ...), custom_call_target="tpu_custom_call" | custom-call | tf_op jit(solution)/shard_map/mixer/pallas_call | solution.py:553
  115.6 0.7 copy.23
Async XLA Ops:
  0.0 0.8 copy-start.12
  0.0 0.8 copy-start.14
  0.0 0.8 copy-start.15
  0.8 1.0 copy-start
  1.8 0.9 copy-start.1
  2.7 0.9 copy-start.2
  3.7 0.8 copy-start.3
  4.5 0.8 copy-start.4
  5.4 0.8 copy-start.5
  6.2 0.8 copy-start.6
  7.0 0.8 copy-start.7
  7.9 0.8 copy-start.8
  8.7 0.8 copy-start.9
  9.6 0.8 copy-start.10
  10.4 0.8 copy-start.11
  11.2 0.7 copy-start.13

commit v3 on v2

v3 whole, which is shorter than its diff:
```python
import functools

import jax
import jax.numpy as jnp
import numpy as np
from jax import lax
from jax.experimental import pallas as pl
from jax.experimental.pallas import tpu as pltpu
from jax.sharding import PartitionSpec as P

HEAD_DIM = 128
CONV_WIDTH = 2048
KERNEL = 31
EPS = 1e-06
THETA = 10000.0
ROWS = 512
ORDER = (0, 1, 7, 2, 6, 3, 5, 4)
BF = jnp.bfloat16
F32 = jnp.float32
MESH = pl.DeviceIdType.MESH
VM = pl.BlockSpec(memory_space=pltpu.VMEM)
HBM = pl.BlockSpec(memory_space=pltpu.HBM)
SM = pl.BlockSpec(memory_space=pltpu.SMEM)
MIB = 1 << 20


def place():
    sp, tp = lax.axis_index("sp"), lax.axis_index("tp")
    return tp // 2, sp % 4, sp // 4, tp % 2


def at(x, y, z, c):
    return (z * 4 + y, x * 2 + c)


def when(cond, f):
    if cond is None:
        f()
    else:
        pl.when(cond)(f)


class Post:
    def __init__(self, send_sems, recv_sems):
        self.ss, self.rs = send_sems, recv_sems
        self.sent, self.ids = [], {}

    def key(self, name):
        return self.rs.at[self.ids.setdefault(name, len(self.ids))]

    def send(self, name, src, dst, to, cond=None, recv=None):
        sem = self.ss.at[len(self.sent)]
        recv = self.key(name) if recv is None else recv

        def make():
            return pltpu.make_async_remote_copy(
                src_ref=src, dst_ref=dst, send_sem=sem, recv_sem=recv, device_id=to, device_id_type=MESH
            )

        self.sent.append((make, cond))
        when(cond, lambda: make().start())

    def local(self, name, src, dst, cond=None, recv=None):
        recv = self.key(name) if recv is None else recv
        when(cond, lambda: pltpu.make_async_copy(src, dst, recv).start())

    def recv(self, name, ref, cond=None, recv=None):
        recv = self.key(name) if recv is None else recv
        when(cond, lambda: pltpu.make_async_copy(ref, ref, recv).wait())

    def finish(self):
        for make, cond in self.sent:
            when(cond, lambda: make().wait_send())


def greet(peers):
    barrier = pltpu.get_barrier_semaphore()
    for peer in peers:
        pl.semaphore_signal(barrier, inc=1, device_id=peer, device_id_type=MESH)
    pl.semaphore_wait(barrier, len(peers))


def rows_at(start, size, unit=16):
    return pl.ds(pl.multiple_of(start, unit), size)


def cols_at(start, size):
    return pl.ds(pl.multiple_of(start, 128), size)


def dot(a, b, dims=((1,), (0,))):
    return lax.dot_general(a, b, (dims, ((), ())), preferred_element_type=F32)


def log_sigmoid(decay):
    t = jnp.exp(-decay)
    s = t / (2.0 + t)
    square = s * s
    series = jnp.full_like(s, 1.0 / 15)
    for n in (13, 11, 9, 7, 5, 3, 1):
        series = series * square + 1.0 / n
    return -2.0 * s * series


def mixer_kernel(
    xin, wq, wk, wv, wg, wa, wb, wr, wc, dk_in, v0, v1, v2, v3, v4, gain_in, cos_in, sin_in, base_in, df, db, out,
    xg, nrm, wt, wo, dk, pv, gain, cosine, sine, base, dec, decp, qs, inner, gs, us, st, sp, chip, sg, halo,
    pad, filt, stat, stats, both, part, acc,
    a2m, a2p, am, ap, ta, u, ua, b2m, b2p, bm, bp, bo, tb, v, vb, ss, rs,
):
    pv_in = (v0, v1, v2, v3, v4)
    x, y, z, c = place()
    n = z * 2 + c
    ct, yl = y // 2, y % 2
    xp, xm, x2 = (x + 1) % 4, (x + 3) % 4, (x + 2) % 4
    yp, ym, y2 = (y + 1) % 4, (y + 3) % 4, (y + 2) % 4
    zp, zm = (z + 1) % 8, (z + 7) % 8
    own = ct == c
    other = ct != c
    post = Post(ss, rs)
    partner = at(x, y, z, 1 - c)
    post.local("gain", gain_in, gain)
    post.local("cos", cos_in, cosine)
    post.local("sin", sin_in, sine)
    post.local("base", base_in, base)
    line = [(dz, (z + dz) % 8) for dz in range(1, 8)]
    greet(
        [at(q, y, z, k) for q in (xp, xm) for k in (0, 1)]
        + [at(x, q, z, k) for q in (yp, ym, y2) for k in (0, 1)]
        + [at(x, y, zp, c), at(x, y, zm, c), partner]
    )

    def xblock(yy, half, r0, rn, col, width):
        return xg.at[rows_at((yy % 2) * 256 + half * 128 + r0, rn), cols_at(col, width)]

    s = z * 4 + y
    post.key("w0"), post.key("w1")
    wsem = rs.at[post.ids["w0"] + yl]

    def wstart(near):
        j = 1 - yl if near else yl
        to = at(x, 2 * c + j, z, ct)
        for m, w in enumerate((wq, wk, wv, wg, wa, wb)):
            src, dst = w.at[:, cols_at(j * 128, 128)], wt.at[rows_at(s * 128, 128), pl.ds(m * 128, 128)]
            if near:
                post.send("w", src, dst, to, None, wsem)
            else:
                post.local("w", src, dst, own, wsem)
                post.send("w", src, dst, to, other, wsem)

    def ostart(near):
        j = 1 - yl if near else yl
        to = at(x, 2 * c + j, z, ct)
        for m, w in enumerate((wr, wc)):
            src, dst = w.at[rows_at(j * 128, 128), :], wo.at[pl.ds(m * 128, 128), cols_at(s * 128, 128)]
            if near:
                post.send("o", src, dst, to)
            else:
                post.local("o", src, dst, own)
                post.send("o", src, dst, to, other)

    wstart(True)
    mine = (x * 2 + c) * 512
    for half, name, ends in ((1, "x2", ((x, yp, "m"), (x, ym, "p"))), (0, "x1", ((xp, y, "m"), (xm, y, "p")))):
        src, dst = xin.at[pl.ds(half * 128, 128), :], xblock(y, half, 0, 128, mine, 512)
        for qx, qy, d in ends:
            post.send(name + d, src, dst, at(qx, qy, z, ct))
        post.send(name + "l", src, dst, partner, other)
        post.local(name + "s", src, dst, own)
    wstart(False)
    for name, ref, dst in (("dk", dk_in, dk), *((("v", i), r, pv.at[i]) for i, r in enumerate(pv_in))):
        src = ref.at[:, cols_at(yl * 128, 128)]
        post.send(name, src, dst, partner, own)
        post.local(name, src, dst, own)
    decp[0:1, :] = log_sigmoid(jnp.full((1, 128), df[yl], F32))
    decp[1:2, :] = log_sigmoid(jnp.full((1, 128), db[yl], F32))

    first = (yl + c + ct) % 2

    def wrows(zz, i, r0=0, rn=128):
        sub = first if i == 0 else 1 - first
        return wt.at[rows_at((zz * 4 + 2 * c + sub) * 128 + r0, rn), :]

    def zsend(zz, i, r, d, r0=0, rn=128):
        ref = wrows(zz, i, r0, rn)
        post.send(("z", d, r, i), ref, ref, at(x, y, zp if d == "m" else zm, c))

    def zpass(zz, i, rel, r0=0, rn=128):
        ref = wrows(zz, i, r0, rn)
        post.send(("zp", rel, i, r0), ref, ref, partner)

    def ocols(zz, i, core=c):
        return wo.at[:, cols_at((zz * 4 + 2 * core + i) * 128, 128)]

    def osend(zz, i, r, d):
        post.send(("o", d, r, i), ocols(zz, i), ocols(zz, i), at(x, y, zp if d == "m" else zm, c))

    def opass(zz, i, rel):
        post.send(("op", rel, i), ocols(zz, i), ocols(zz, i), partner)

    def wfirst(i):
        post.recv("w", wrows(z, i), None, rs.at[post.ids["w0"] + (first if i == 0 else 1 - first)])
        for d in ("m", "p"):
            zsend(z, i, 1, d)
        zpass(z, i, 0)

    wfirst(0)
    cm, cp, c2 = ym // 2 == c, yp // 2 == c, y2 // 2 == c
    post.recv("x1m", xblock(y, 0, 0, 128, xm * 1024, 1024), own)
    ref = xblock(y, 0, 0, 64, xm * 1024, 1024)
    post.send("x1m2", ref, ref, at(xp, y, z, c), own)
    post.recv("x1p", xblock(y, 0, 0, 128, xp * 1024, 1024), own)
    ref = xblock(y, 0, 64, 64, xp * 1024, 1024)
    post.send("x1p2", ref, ref, at(xm, y, z, c), own)
    post.recv("x2m", xblock(ym, 1, 0, 128, x * 1024, 1024), cm)
    ref = xblock(ym, 1, 0, 64, x * 1024, 1024)
    post.send("x2m2", ref, ref, at(x, yp, z, c), cm)
    post.recv("x2p", xblock(yp, 1, 0, 128, x * 1024, 1024), cp)
    ref = xblock(yp, 1, 64, 64, x * 1024, 1024)
    post.send("x2p2", ref, ref, at(x, ym, z, c), cp)

    for name, half in (("x1", 0), ("x2", 1)):
        post.recv(name + "s", xblock(y, half, 0, 128, mine, 512), own)
        post.recv(name + "l", xblock(y, half, 0, 128, (x * 2 + 1 - c) * 512, 512), own)
    post.recv("x1m2", xblock(y, 0, 0, 64, x2 * 1024, 1024), own)
    post.recv("x1p2", xblock(y, 0, 64, 64, x2 * 1024, 1024), own)
    for i in (0, 1):
        ref = xblock(y, 0, i * 64, 64, 0, 4096)
        post.send(("x3m", i), ref, ref, at(x, yp, z, c), own)
    for i in (1, 0):
        ref = xblock(y, 0, i * 64, 64, 0, 4096)
        post.send(("x3p", i), ref, ref, at(x, ym, z, c), own)
    wfirst(1)
    post.recv("x2m2", xblock(y2, 1, 0, 64, x * 1024, 1024), c2)
    post.recv("x2p2", xblock(y2, 1, 64, 64, x * 1024, 1024), c2)

    def x4(qx, k):
        return xblock(k, 1, 0, 128, qx * 1024, 1024)

    for d, to, order in (("m", xp, (0, 1)), ("p", xm, (1, 0))):
        for k in order:
            post.send(("x4" + d, k), x4(x, k), x4(x, k), at(to, y, z, c))
    ostart(True)
    ostart(False)
    post.send("dec", decp, dec, partner, own)

    def zstep(r, parts=(0, 1)):
        for i in parts:
            for d in ("m", "p"):
                zz = (z - r) % 8 if d == "m" else (z + r) % 8
                post.recv(("z", d, r, i), wrows(zz, i))
                if r < 3:
                    zsend(zz, i, r + 1, d)
                else:
                    zsend(zz, i, 4, d, 0 if d == "m" else 64, 64)
                zpass(zz, i, -r % 8 if d == "m" else r)

    def ostep(r, i):
        for d in ("m", "p"):
            zz = (z - r) % 8 if d == "m" else (z + r) % 8
            if r == 4 and i != (d == "p"):
                continue
            post.recv(("o", d, r, i), ocols(zz, i))
            if r < 3 or (r == 3 and i == (d == "p")):
                osend(zz, i, r + 1, d)
            opass(zz, i, -r % 8 if d == "m" else r)

    zstep(1)
    post.recv(("x3m", 0), xblock(ym, 0, 0, 64, 0, 4096), cm)
    ref = xblock(ym, 0, 0, 64, 0, 4096)
    post.send("x3m2", ref, ref, at(x, yp, z, c), cm)
    post.recv(("x3p", 1), xblock(yp, 0, 64, 64, 0, 4096), cp)
    ref = xblock(yp, 0, 64, 64, 0, 4096)
    post.send("x3p2", ref, ref, at(x, ym, z, c), cp)
    post.recv(("x4m", 0), x4(xm, 0))
    post.send("x4m2", x4(xm, 0), x4(xm, 0), at(xp, y, z, c))
    post.recv(("x4p", 1), x4(xp, 1))
    post.send("x4p2", x4(xp, 1), x4(xp, 1), at(xm, y, z, c))
    zstep(2)
    post.recv("o", wo.at[:, cols_at((z * 4 + 2 * c) * 128, 256)])
    zstep(3, (0,))
    post.recv(("x3m", 1), xblock(ym, 0, 64, 64, 0, 4096), cm)
    post.recv(("x3p", 0), xblock(yp, 0, 0, 64, 0, 4096), cp)
    post.recv("x3m2", xblock(y2, 0, 0, 64, 0, 4096), c2)
    post.recv("x3p2", xblock(y2, 0, 64, 64, 0, 4096), c2)
    post.recv(("x4m", 1), x4(xm, 1))
    post.recv(("x4p", 0), x4(xp, 0))
    post.recv("x4m2", x4(x2, 0))
    post.recv("x4p2", x4(x2, 1))
    for name, ref in (("gain", gain), ("cos", cosine), ("sin", sine), ("base", base), ("dk", dk), *((("v", i), pv.at[i]) for i in range(5))):
        post.recv(name, ref)

    @pl.loop(0, ROWS // 128)
    def _(i):
        rows = rows_at(i * 128, 128)
        square = jnp.zeros((128, 128), F32)
        for k in range(32):
            piece = xg[rows, k * 128 : k * 128 + 128].astype(F32)
            square = square + piece * piece
        scale = lax.rsqrt(jnp.sum(square, axis=1, keepdims=True) / 4096 + EPS)
        for k in range(32):
            cols = slice(k * 128, k * 128 + 128)
            nrm[rows, cols] = (xg[rows, cols].astype(F32) * scale * gain[:, cols]).astype(BF)

    zstep(3, (1,))
    for i in (0, 1):
        for d in ("m", "p"):
            osend(z, i, 1, d)
    for i in (0, 1):
        opass(z, i, 0)

    def zpassed(rel):
        zz = (z + rel) % 8
        for i in (0, 1):
            sub = 1 - first if i == 0 else first
            for r0, rn in ((0, 64), (64, 64)) if rel == 4 else ((0, 128),):
                row = (zz * 4 + 2 * (1 - c) + sub) * 128 + r0
                post.recv(("zp", rel, i, r0), wt.at[rows_at(row, rn), :])

    def project(rel):
        start = ((z + rel) % 8) * 512
        return dot(nrm[:, cols_at(start, 512)], wt[rows_at(start, 512), :])

    far = (z + 4) % 8

    def projects(*rels):
        for rel in rels:
            zpassed(rel)
            acc[...] = project(rel) if rel == 0 else acc[...] + project(rel)

    projects(0, 1, 7, 2, 6)
    for i in (0, 1):
        for d, r0 in (("m", 0), ("p", 64)):
            post.recv(("z", d, 4, i), wrows(far, i, r0, 64))
            zpass(far, i, 4, r0, 64)
        projects(3 if i == 0 else 5)
    ostep(1, 0)
    post.recv("dec", dec, other)

    @pl.when(own)
    def _():
        dec[...] = decp[...]

    zpassed(4)
    proj = (acc[...] + project(4)).astype(BF)
    ostep(1, 1)
    cb, sb = base[n][:, 0:128], base[n][:, 128:256]
    cosine[...], sine[...] = cosine[...] * cb - sine[...] * sb, sine[...] * cb + cosine[...] * sb

    def turn(rows):
        wide = rows.astype(F32)
        return (wide * cosine[...] + pltpu.roll(wide, 64, axis=1) * sine[...]).astype(BF)

    keys, values = turn(proj[:, 128:256]), proj[:, 256:384]
    us[...] = (proj[:, 512:640].astype(F32) * jax.nn.sigmoid(proj[:, 640:768].astype(F32))).astype(BF)
    after, before = (n + 1) % 16, (n + 15) % 16
    post.send("ht", us.at[pl.ds(ROWS - 16, 16), :], halo.at[0], at(x, y, after // 2, after % 2))
    post.send("hh", us.at[pl.ds(0, 16), :], halo.at[1], at(x, y, before // 2, before % 2))
    lf, lb = dec[0:1, :], dec[1:2, :]
    place_ = lax.broadcasted_iota(jnp.int32, (ROWS, 128), 0).astype(F32)
    wide = keys.astype(F32)
    st[0] = dot((wide * jnp.exp(lb * place_)).astype(BF), values, ((0,), (0,))).astype(BF)
    st[1] = dot((wide * jnp.exp(lf * (ROWS - 1.0 - place_))).astype(BF), values, ((0,), (0,))).astype(BF)
    post.send("sp", st, sp, partner)
    queries = turn(proj[:, 0:128])
    gs[...] = proj[:, 384:512]
    qs[...] = queries
    f1, b1 = lf[:, 0:1], lb[:, 0:1]
    for i in range(ROWS // 128):
        rows = slice(i * 128, i * 128 + 128)
        gap = (
            lax.broadcasted_iota(jnp.int32, (128, ROWS), 0)
            + i * 128
            - lax.broadcasted_iota(jnp.int32, (128, ROWS), 1)
        ).astype(F32)
        decay = jnp.exp(jnp.where(gap >= 0, f1 * gap, -b1 * gap))
        scores = dot(queries[rows], keys, ((1,), (1,))) * decay
        inner[rows, :] = dot(scores.astype(BF), values)
    post.recv("sp", sp)
    span = jnp.exp(jnp.where(c == 1, lf, lb) * float(ROWS))
    chip[...] = (st[c].astype(F32) + span * sp[c].astype(F32)).astype(BF)

    def meant(a, b):
        return (a < b) == (c == 1)

    for dz, q in line:
        post.send(("st", dz), chip, sg.at[z], at(x, y, q, c), meant(z, q))
    ostep(2, 0)

    post.recv("ht", halo.at[0])
    post.recv("hh", halo.at[1])
    pad[0:16, :] = jnp.where(n > 0, halo[0].astype(F32), 0.0)
    pad[16 : 16 + ROWS, :] = us[...].astype(F32)
    pad[16 + ROWS :, :] = jnp.where(n < 15, halo[1].astype(F32), 0.0)
    lane = lax.broadcasted_iota(jnp.int32, (128, 128), 1)
    for i in range(ROWS // 128):
        filtered = jnp.broadcast_to(pv[0], (128, 128))
        for t in range(KERNEL):
            filtered = filtered + dk[t : t + 1, :] * pad[i * 128 + t + 1 : i * 128 + t + 129, :]
        filt[i * 128 : i * 128 + 128, :] = filtered
        total = jnp.sum(filtered, axis=1, keepdims=True)
        square = jnp.sum(filtered * filtered, axis=1, keepdims=True)
        tile = jnp.where(lane == 0, total, jnp.where(lane == 1, square, 0.0))
        stat[:, i * 128 : i * 128 + 128] = tile.T[0:8, :]
    ostep(2, 1)
    me = x * 4 + y
    for i in range(4):
        for j in range(4):
            if i or j:
                post.send("stats", stat, stats.at[me], at((x + i) % 4, (y + j) % 4, z, c))
    stats[pl.ds(me, 1)] = stat[...][None]
    for dz, q in line:
        source = (z - dz) % 8
        slot = sg.at[source]
        post.recv(("st", dz), slot, meant(source, z))
        post.send(("ss", dz), slot, slot, partner, meant(source, z))
    ostep(3, 0)
    sg[pl.ds(z, 1)] = jnp.zeros((1, 128, 128), BF)
    for dz, q in line:
        source = (z - dz) % 8
        post.recv(("ss", dz), sg.at[source], jnp.logical_not(meant(source, z)))
    enter_f, enter_b = jnp.zeros((128, 128), F32), jnp.zeros((128, 128), F32)
    for j in range(8):
        state = sg[j].astype(F32)
        ahead, behind = z - 1 - j, j - z - 1
        wf = jnp.exp(lf * (2 * ROWS * jnp.maximum(ahead, 0)).astype(F32))
        wb_ = jnp.exp(lb * (2 * ROWS * jnp.maximum(behind, 0)).astype(F32))
        enter_f = enter_f + jnp.where(ahead >= 0, wf, 0.0) * state
        enter_b = enter_b + jnp.where(behind >= 0, wb_, 0.0) * state
    enter_f = jnp.where(c == 1, jnp.exp(lf * float(ROWS)) * enter_f + sp[1].astype(F32), enter_f)
    enter_b = jnp.where(c == 0, jnp.exp(lb * float(ROWS)) * enter_b + sp[0].astype(F32), enter_b)
    wide = qs[...].astype(F32)
    retained = inner[...]
    retained = retained + dot((wide * jnp.exp(lf * (place_ + 1.0))).astype(BF), enter_f.astype(BF))
    retained = retained + dot((wide * jnp.exp(lb * (ROWS - place_))).astype(BF), enter_b.astype(BF))
    mean = jnp.mean(retained, axis=-1, keepdims=True)
    centered = retained - mean
    variance = jnp.mean(centered * centered, axis=-1, keepdims=True)
    scaled = centered * lax.rsqrt(variance + EPS) * pv[3] + pv[4]
    both[:, 0:128] = (jax.nn.silu(gs[...].astype(F32)) * scaled).astype(BF)

    ostep(3, 1)
    post.recv("stats", stats.at[pl.ds(0, 15)])
    total = stats[0]
    for j in range(1, 16):
        total = total + stats[j]
    for i in range(ROWS // 128):
        rows = slice(i * 128, i * 128 + 128)
        tall = jnp.concatenate([total[:, rows], jnp.zeros((120, 128), F32)], axis=0).T
        mean = tall[:, 0:1] / CONV_WIDTH
        variance = tall[:, 1:2] / CONV_WIDTH - mean * mean
        leveled = (filt[rows, :] - mean) * lax.rsqrt(variance + EPS) * pv[1] + pv[2]
        both[rows, 128:256] = jax.nn.silu(leveled).astype(BF)
    def out_part(slots):
        for k in slots:
            zz = (z + ORDER[k]) % 8
            for i in (0, 1):
                post.recv(("op", ORDER[k], i), ocols(zz, i, 1 - c))
            cols = slice(k * 512, k * 512 + 512)
            value = dot(both[...], wo[:, cols_at(zz * 512, 512)])
            part[:, :, :, :, cols] = value.astype(BF).reshape(2, 4, 2, 32, 512)

    to_xp, to_xm = at(xp, y, z, c), at(xm, y, z, c)
    c1p, c1m = cp, cm
    right = pl.ds(2560, 1536)
    groups = (pl.ds(0, 1536), pl.ds(1536, 1024))

    def add(a, b):
        return (a.astype(F32) + b.astype(F32)).astype(BF)

    def afirst(g):
        cols = groups[g]
        post.send(("a2m", g), part.at[0, x2, :, :, cols], a2m.at[:, :, cols], to_xp)
        post.send(("a2p", g), part.at[1, x2, :, :, cols], a2p.at[:, :, cols], to_xm)
        post.send(("am1", g), part.at[1, xp, :, :, cols], am.at[1, :, :, cols], to_xp)
        post.send(("ap0", g), part.at[0, xm, :, :, cols], ap.at[0, :, :, cols], to_xm)

    def asecond(g):
        cols = groups[g]
        post.recv(("a2m", g), a2m.at[:, :, cols])
        ta[0, :, :, cols] = add(a2m[:, :, cols], part[0, xp, :, :, cols])
        post.send(("am0", g), ta.at[0, :, :, cols], am.at[0, :, :, cols], to_xp)
        post.recv(("a2p", g), a2p.at[:, :, cols])
        ta[1, :, :, cols] = add(a2p[:, :, cols], part[1, xm, :, :, cols])
        post.send(("ap1", g), ta.at[1, :, :, cols], ap.at[1, :, :, cols], to_xm)

    def athird(g):
        cols = groups[g]
        for name, ref in (("am1", am.at[1]), ("ap0", ap.at[0]), ("am0", am.at[0]), ("ap1", ap.at[1])):
            post.recv((name, g), ref.at[:, :, cols])
        for k in (0, 1):
            value = part[k, x, :, :, cols].astype(F32) + am[k, :, :, cols].astype(F32)
            u[k, :, :, cols] = (value + ap[k, :, :, cols].astype(F32)).astype(BF)
        for k in (0, 1):
            for k2 in (0, 1):
                q = 2 * c + k
                here = (q == y) & (k2 == c)
                src, dst = u.at[k, k2, :, cols], ua.at[y, :, cols]
                post.send(("ua", g), src, dst, at(x, q, z, k2), jnp.logical_not(here))
                post.local(("ua", g), src, dst, here)

    def alast(g):
        cols = groups[g]
        post.recv(("ua", g), ua.at[:, :, cols])
        for k in range(cols.start // 512, (cols.start + cols.size) // 512):
            piece = slice(k * 512, k * 512 + 512)
            value = ua[0, :, piece].astype(F32)
            for q in (1, 2, 3):
                value = value + ua[q, :, piece].astype(F32)
            out[:, cols_at(((z + ORDER[k]) % 8) * 512, 512)] = value.astype(BF)

    def pb(yy, q0, k):
        return part.at[yy % 2, pl.ds(q0, 2), k, :, right]

    out_part((0, 1, 2))
    afirst(0)
    out_part((3, 4))
    afirst(1)
    for i in (0, 1):
        ostep(4, i)
    out_part((5, 6, 7))
    for k in (0, 1):
        post.send("b2m", pb(y2, 0, k), b2m.at[k], at(x, yp, z, c), c2)
        post.send("b2p", pb(y2, 2, k), b2p.at[k], at(x, ym, z, c), c2)
    for k in (0, 1):
        post.send("bm1", pb(yp, 2, k), bm.at[pl.ds(2, 2)], at(x, yp, z, k), c1p)
        post.send("bp0", pb(ym, 0, k), bp.at[pl.ds(0, 2)], at(x, ym, z, k), c1m)
    post.send("bo", part.at[y % 2, :, 1 - c, :, right], bo, partner, own)
    asecond(0)
    asecond(1)
    post.recv("b2m", b2m, c1p)

    @pl.when(c1p)
    def _():
        for k in (0, 1):
            tb[0, k] = add(b2m[k], part[yp % 2, 0:2, k, :, right])

    for k in (0, 1):
        post.send("bm0", tb.at[0, k], bm.at[pl.ds(0, 2)], at(x, yp, z, k), c1p)
    post.recv("b2p", b2p, c1m)

    @pl.when(c1m)
    def _():
        for k in (0, 1):
            tb[1, k] = add(b2p[k], part[ym % 2, 2:4, k, :, right])

    for k in (0, 1):
        post.send("bp1", tb.at[1, k], bp.at[pl.ds(2, 2)], at(x, ym, z, k), c1m)

    @pl.when(own)
    def _():
        bo[...] = part[y % 2, :, c, :, right]

    athird(0)
    post.recv("bm1", bm.at[pl.ds(2, 2)])
    post.recv("bp0", bp.at[pl.ds(0, 2)])
    post.recv("bo", bo, other)
    post.recv("bm0", bm.at[pl.ds(0, 2)])
    post.recv("bp1", bp.at[pl.ds(2, 2)])
    for q in range(4):
        v[q] = (bm[q].astype(F32) + bp[q].astype(F32) + bo[q].astype(F32)).astype(BF)
    for q in (x2, xp, xm):
        post.send("vb", v.at[q], vb.at[x], at(q, y, z, c))
    vb[pl.ds(x, 1)] = v[pl.ds(x, 1)]
    athird(1)
    alast(0)
    post.recv("vb", vb.at[pl.ds(0, 3)])
    for k in (5, 6, 7):
        piece = slice((k - 5) * 512, (k - 5) * 512 + 512)
        value = vb[0, :, piece].astype(F32)
        for q in (1, 2, 3):
            value = value + vb[q, :, piece].astype(F32)
        out[:, cols_at(((z + ORDER[k]) % 8) * 512, 512)] = value.astype(BF)
    alast(1)
    post.finish()


def table():
    half = HEAD_DIM // 2
    inverse = np.tile(THETA ** (-np.arange(half) / half), 2)
    sign = np.repeat([-1.0, 1.0], half)
    near = np.arange(ROWS)[:, None] * inverse
    far = np.arange(16)[:, None] * ROWS * inverse
    base = np.concatenate([np.cos(far), sign * np.sin(far)], axis=1)
    return [a.astype(np.float32) for a in (np.cos(near), sign * np.sin(near), base[:, None])]


def shards(
    hidden_states,
    norm_gain,
    query_weight,
    key_weight,
    value_weight,
    output_gate_weight,
    unit_input_weight,
    unit_gate_weight,
    decay_forward,
    decay_backward,
    group_gain,
    group_bias,
    depth_kernel,
    depth_bias,
    channel_gain,
    channel_bias,
    retention_out_weight,
    convolution_out_weight,
):
    vectors = (depth_bias, channel_gain, channel_bias, group_gain, group_bias)
    wide = lambda *shape: pltpu.VMEM((*shape, 2560), BF)
    narrow = lambda *shape: pltpu.VMEM((*shape, 1536), BF)
    small = lambda dtype: pltpu.VMEM((ROWS, 128), dtype)
    return pl.pallas_call(
        mixer_kernel,
        name="mixer",
        out_shape=jax.ShapeDtypeStruct((32, 4096), BF),
        in_specs=[HBM] * 19 + [SM] * 2,
        out_specs=VM,
        scratch_shapes=[
            pltpu.VMEM((ROWS, 4096), BF),
            pltpu.VMEM((ROWS, 4096), BF),
            pltpu.VMEM((4096, 768), BF),
            pltpu.VMEM((256, 4096), BF),
            pltpu.VMEM((KERNEL, 128), F32),
            pltpu.VMEM((5, 1, 128), F32),
            pltpu.VMEM((1, 4096), F32),
            small(F32),
            small(F32),
            pltpu.VMEM((16, 1, 256), F32),
            pltpu.VMEM((8, 128), F32),
            pltpu.VMEM((8, 128), F32),
            small(BF),
            small(F32),
            small(BF),
            small(BF),
            pltpu.VMEM((2, 128, 128), BF),
            pltpu.VMEM((2, 128, 128), BF),
            pltpu.VMEM((128, 128), BF),
            pltpu.VMEM((8, 128, 128), BF),
            pltpu.VMEM((2, 16, 128), BF),
            pltpu.VMEM((ROWS + 32, 128), F32),
            small(F32),
            pltpu.VMEM((8, ROWS), F32),
            pltpu.VMEM((16, 8, ROWS), F32),
            pltpu.VMEM((ROWS, 256), BF),
            pltpu.VMEM((2, 4, 2, 32, 4096), BF),
            pltpu.VMEM((ROWS, 768), F32),
            wide(2, 32),
            wide(2, 32),
            wide(2, 2, 32),
            wide(2, 2, 32),
            wide(2, 2, 32),
            wide(2, 2, 32),
            wide(4, 32),
            narrow(2, 2, 32),
            narrow(2, 2, 32),
            narrow(4, 32),
            narrow(4, 32),
            narrow(4, 32),
            narrow(2, 2, 2, 32),
            narrow(4, 32),
            narrow(4, 32),
            pltpu.SemaphoreType.DMA((230,)),
            pltpu.SemaphoreType.DMA((180,)),
        ],
        compiler_params=pltpu.CompilerParams(
            collective_id=0, has_side_effects=True, vmem_limit_bytes=67043328
        ),
    )(
        hidden_states,
        query_weight,
        key_weight,
        value_weight,
        output_gate_weight,
        unit_input_weight,
        unit_gate_weight,
        retention_out_weight,
        convolution_out_weight,
        depth_kernel,
        *(vector.reshape(1, -1) for vector in vectors),
        norm_gain.reshape(1, -1),
        *table(),
        decay_forward,
        decay_backward,
    )


def solution(mesh):
    split = P("sp", "tp")
    placed = (
        (split, P())
        + (split,) * 6
        + (P("tp"),) * 4
        + (P(None, "tp"),)
        + (P("tp"),) * 3
        + (P("tp", "sp"),) * 2
    )
    return jax.shard_map(
        shards, mesh=mesh, in_specs=placed, out_specs=P(("sp", "tp"), None), check_vma=False
    )
```

time: 117 us -> 100 us (0.85)
  local copies, waits for them, and re-layouts: 12.5 us -> 1.67 us
  Pallas kernels: 104 us -> 98.4 us
    unnamed x33 -> x1, local copies, waits for them, and re-layouts: 11.7 us -> 1.67 us
    pallas_call x1, Pallas kernels: 104 us -> 98.4 us  [shards(): pl.pallas_call(mixer_kernel, name='mixer', out_shape=jax.ShapeDtypeStruct...]
where the time goes in v3:
time: 100 us
  Pallas kernels  98.4 us (98%)
  local copies, waits for them, and re-layouts  1.67 us (2%)
    pallas_call x1, Pallas kernels, shards(): pl.pallas_call(mixer_kernel, name='mixer', out_shape=jax.ShapeDtypeStruct...  98.4 us

profile of v3, /device:TPU:1, one launch (start us, length us, event | category | flops | bytes accessed | tf_op | source)
XLA Modules:
  0.0 100.1 jit_solution(9170172558401555658)
XLA Ops:
  0.0 98.4 %mixer.1 = bf16[32,4096]{1,0:T(8,128)(2,1)} custom-call(bf16[256,512]{1,0:T(8,128)(2,1)} %xin.1, bf16[128,256]{1,0:T(8,128)(2,1)} %wq.1, bf16[128,256]{1,0:T(8,128)(2,1)} %wk.1, bf16[128,256]{1,0:T(8,128)(2,1)} %wv.1, bf16[128,256]{1,0:T(8,128)(2,1)} %wg.1, bf16[128,256]{1,0:T(8,128)(2,1)} %wa.1, bf16[128,256]{1,0:T(8,128)(2,1)} %wb.1, bf16[256,128]{1,0:T(8,128)(2,1)} %wr.1, ...), custom_call_target="tpu_custom_call" | custom-call | tf_op jit(solution)/shard_map/mixer/pallas_call | solution.py:612
  98.4 1.7 %copy.23 = bf16[32,4096]{1,0:T(8,128)(2,1)} copy(bf16[32,4096]{1,0:T(8,128)(2,1)} %mixer.1) | data formatting | bytes 524288

commit v4 on v3

--- a/solution.py
+++ b/solution.py
@@ -14,6 +14,7 @@
 EPS = 1e-06
 THETA = 10000.0
 ROWS = 512
+SPLIT = 96
 ORDER = (0, 1, 7, 2, 6, 3, 5, 4)
 BF = jnp.bfloat16
 F32 = jnp.float32
@@ -103,8 +104,8 @@
 
 
 def mixer_kernel(
-    xin, wq, wk, wv, wg, wa, wb, wr, wc, dk_in, v0, v1, v2, v3, v4, gain_in, cos_in, sin_in, base_in, df, db, out,
-    xg, nrm, wt, wo, dk, pv, gain, cosine, sine, base, dec, decp, qs, inner, gs, us, st, sp, chip, sg, halo,
+    xin, w0, w1, w2, w3, w4, w5, wr, wc, dk_in, v0, v1, v2, v3, v4, gain_in, cos_in, sin_in, base_in, df, db, out,
+    xin_v, w_v, wr_v, wc_v, xg, nrm, wt, wo, dk, pv, gain, cosine, sine, base, dec, decp, qs, inner, gs, us, st, sp, chip, sg, halo,
     pad, filt, stat, stats, both, part, acc,
     a2m, a2p, am, ap, ta, u, ua, b2m, b2p, bm, bp, bo, tb, v, vb, ss, rs,
 ):
@@ -115,10 +116,25 @@
     xp, xm, x2 = (x + 1) % 4, (x + 3) % 4, (x + 2) % 4
     yp, ym, y2 = (y + 1) % 4, (y + 3) % 4, (y + 2) % 4
     zp, zm = (z + 1) % 8, (z + 7) % 8
+    post = Post(ss, rs)
+    partner = at(x, y, z, 1 - c)
+    loads = list(zip((xin, w0, w1, w2, w3, w4, w5, wr, wc), (xin_v, *(w_v.at[i] for i in range(6)), wr_v, wc_v)))
+    for i, (src, dst) in enumerate(loads):
+        post.local(("load", i), src, dst)
     own = ct == c
     other = ct != c
-    post = Post(ss, rs)
-    partner = at(x, y, z, 1 - c)
+    mine = (x * 2 + c) * 512
+    s = z * 4 + y
+    for p in (0, 1):
+        post.key(("w", p, 0)), post.key(("w", p, 1))
+
+    def wsem(p, sub):
+        return rs.at[post.ids[("w", p, 0)] + sub]
+
+    group_cols = (pl.ds(0, 512), pl.ds(512, 256))
+    for m, w in enumerate((w0, w1, w2, w3, w4, w5)):
+        src, dst = w.at[:, cols_at(yl * 128, 128)], wt.at[rows_at(s * 128, 128), pl.ds(m * 128, 128)]
+        post.local("w", src, dst, own, wsem(m // 4, yl))
     post.local("gain", gain_in, gain)
     post.local("cos", cos_in, cosine)
     post.local("sin", sin_in, sine)
@@ -131,43 +147,43 @@
     )
 
     def xblock(yy, half, r0, rn, col, width):
-        return xg.at[rows_at((yy % 2) * 256 + half * 128 + r0, rn), cols_at(col, width)]
-
-    s = z * 4 + y
-    post.key("w0"), post.key("w1")
-    wsem = rs.at[post.ids["w0"] + yl]
-
-    def wstart(near):
+        return xg.at[rows_at((yy % 2) * 256 + half * SPLIT + r0, rn), cols_at(col, width)]
+
+    for i, (_, dst) in enumerate(loads):
+        post.recv(("load", i), dst)
+
+    def wstart(near, p):
         j = 1 - yl if near else yl
         to = at(x, 2 * c + j, z, ct)
-        for m, w in enumerate((wq, wk, wv, wg, wa, wb)):
-            src, dst = w.at[:, cols_at(j * 128, 128)], wt.at[rows_at(s * 128, 128), pl.ds(m * 128, 128)]
+        for m in (range(4), range(4, 6))[p]:
+            src, dst = w_v.at[m, :, cols_at(j * 128, 128)], wt.at[rows_at(s * 128, 128), pl.ds(m * 128, 128)]
             if near:
-                post.send("w", src, dst, to, None, wsem)
+                post.send("w", src, dst, to, None, wsem(p, yl))
             else:
-                post.local("w", src, dst, own, wsem)
-                post.send("w", src, dst, to, other, wsem)
+                post.send("w", src, dst, to, other, wsem(p, yl))
 
     def ostart(near):
         j = 1 - yl if near else yl
         to = at(x, 2 * c + j, z, ct)
-        for m, w in enumerate((wr, wc)):
+        for m, (w, w_here) in enumerate(((wr_v, wr), (wc_v, wc))):
             src, dst = w.at[rows_at(j * 128, 128), :], wo.at[pl.ds(m * 128, 128), cols_at(s * 128, 128)]
             if near:
                 post.send("o", src, dst, to)
             else:
-                post.local("o", src, dst, own)
+                post.local("o", w_here.at[rows_at(j * 128, 128), :], dst, own)
                 post.send("o", src, dst, to, other)
 
-    wstart(True)
-    mine = (x * 2 + c) * 512
+    wstart(True, 0)
     for half, name, ends in ((1, "x2", ((x, yp, "m"), (x, ym, "p"))), (0, "x1", ((xp, y, "m"), (xm, y, "p")))):
-        src, dst = xin.at[pl.ds(half * 128, 128), :], xblock(y, half, 0, 128, mine, 512)
+        size = ROWS // 2 - SPLIT if half else SPLIT
+        src, dst = xin_v.at[pl.ds(half * SPLIT, size), :], xblock(y, half, 0, size, mine, 512)
         for qx, qy, d in ends:
             post.send(name + d, src, dst, at(qx, qy, z, ct))
         post.send(name + "l", src, dst, partner, other)
-        post.local(name + "s", src, dst, own)
-    wstart(False)
+        post.local(name + "s", xin.at[pl.ds(half * SPLIT, size), :], dst, own)
+    wstart(False, 0)
+    wstart(True, 1)
+    wstart(False, 1)
     for name, ref, dst in (("dk", dk_in, dk), *((("v", i), r, pv.at[i]) for i, r in enumerate(pv_in))):
         src = ref.at[:, cols_at(yl * 128, 128)]
         post.send(name, src, dst, partner, own)
@@ -177,17 +193,17 @@
 
     first = (yl + c + ct) % 2
 
-    def wrows(zz, i, r0=0, rn=128):
+    def wrows(zz, i, p, r0=0, rn=128):
         sub = first if i == 0 else 1 - first
-        return wt.at[rows_at((zz * 4 + 2 * c + sub) * 128 + r0, rn), :]
-
-    def zsend(zz, i, r, d, r0=0, rn=128):
-        ref = wrows(zz, i, r0, rn)
-        post.send(("z", d, r, i), ref, ref, at(x, y, zp if d == "m" else zm, c))
-
-    def zpass(zz, i, rel, r0=0, rn=128):
-        ref = wrows(zz, i, r0, rn)
-        post.send(("zp", rel, i, r0), ref, ref, partner)
+        return wt.at[rows_at((zz * 4 + 2 * c + sub) * 128 + r0, rn), group_cols[p]]
+
+    def zsend(zz, i, r, d, p, r0=0, rn=128):
+        ref = wrows(zz, i, p, r0, rn)
+        post.send(("z", p, d, r, i), ref, ref, at(x, y, zp if d == "m" else zm, c))
+
+    def zpass(zz, i, rel, p, r0=0, rn=128):
+        ref = wrows(zz, i, p, r0, rn)
+        post.send(("zp", p, rel, i, r0), ref, ref, partner)
 
     def ocols(zz, i, core=c):
         return wo.at[:, cols_at((zz * 4 + 2 * core + i) * 128, 128)]
@@ -198,62 +214,99 @@
     def opass(zz, i, rel):
         post.send(("op", rel, i), ocols(zz, i), ocols(zz, i), partner)
 
-    def wfirst(i):
-        post.recv("w", wrows(z, i), None, rs.at[post.ids["w0"] + (first if i == 0 else 1 - first)])
+    def wfirst(i, p):
+        post.recv("w", wrows(z, i, p), None, wsem(p, first if i == 0 else 1 - first))
         for d in ("m", "p"):
-            zsend(z, i, 1, d)
-        zpass(z, i, 0)
-
-    wfirst(0)
+            zsend(z, i, 1, d, p)
+        zpass(z, i, 0, p)
+
+    def zstep(r, parts, p):
+        for i in parts:
+            for d in ("m", "p"):
+                zz = (z - r) % 8 if d == "m" else (z + r) % 8
+                post.recv(("z", p, d, r, i), wrows(zz, i, p))
+                if r < 3:
+                    zsend(zz, i, r + 1, d, p)
+                else:
+                    zsend(zz, i, 4, d, p, 0 if d == "m" else 64, 64)
+                zpass(zz, i, -r % 8 if d == "m" else r, p)
+
+    far = (z + 4) % 8
+
+    def zfar(i, p):
+        for d, r0 in (("m", 0), ("p", 64)):
+            post.recv(("z", p, d, 4, i), wrows(far, i, p, r0, 64))
+            zpass(far, i, 4, p, r0, 64)
+
+    wfirst(0, 0)
     cm, cp, c2 = ym // 2 == c, yp // 2 == c, y2 // 2 == c
-    post.recv("x1m", xblock(y, 0, 0, 128, xm * 1024, 1024), own)
-    ref = xblock(y, 0, 0, 64, xm * 1024, 1024)
-    post.send("x1m2", ref, ref, at(xp, y, z, c), own)
-    post.recv("x1p", xblock(y, 0, 0, 128, xp * 1024, 1024), own)
-    ref = xblock(y, 0, 64, 64, xp * 1024, 1024)
-    post.send("x1p2", ref, ref, at(xm, y, z, c), own)
-    post.recv("x2m", xblock(ym, 1, 0, 128, x * 1024, 1024), cm)
-    ref = xblock(ym, 1, 0, 64, x * 1024, 1024)
-    post.send("x2m2", ref, ref, at(x, yp, z, c), cm)
-    post.recv("x2p", xblock(yp, 1, 0, 128, x * 1024, 1024), cp)
-    ref = xblock(yp, 1, 64, 64, x * 1024, 1024)
-    post.send("x2p2", ref, ref, at(x, ym, z, c), cp)
-
-    for name, half in (("x1", 0), ("x2", 1)):
-        post.recv(name + "s", xblock(y, half, 0, 128, mine, 512), own)
-        post.recv(name + "l", xblock(y, half, 0, 128, (x * 2 + 1 - c) * 512, 512), own)
-    post.recv("x1m2", xblock(y, 0, 0, 64, x2 * 1024, 1024), own)
-    post.recv("x1p2", xblock(y, 0, 64, 64, x2 * 1024, 1024), own)
-    for i in (0, 1):
-        ref = xblock(y, 0, i * 64, 64, 0, 4096)
-        post.send(("x3m", i), ref, ref, at(x, yp, z, c), own)
-    for i in (1, 0):
-        ref = xblock(y, 0, i * 64, 64, 0, 4096)
-        post.send(("x3p", i), ref, ref, at(x, ym, z, c), own)
-    wfirst(1)
-    post.recv("x2m2", xblock(y2, 1, 0, 64, x * 1024, 1024), c2)
-    post.recv("x2p2", xblock(y2, 1, 64, 64, x * 1024, 1024), c2)
-
-    def x4(qx, k):
-        return xblock(k, 1, 0, 128, qx * 1024, 1024)
-
-    for d, to, order in (("m", xp, (0, 1)), ("p", xm, (1, 0))):
-        for k in order:
-            post.send(("x4" + d, k), x4(x, k), x4(x, k), at(to, y, z, c))
+    near, far_ = SPLIT // 2, (ROWS // 2 - SPLIT) // 2
+
+    def x1(qx, r0=0, rn=SPLIT):
+        return xblock(y, 0, r0, rn, qx * 1024, 1024)
+
+    def x2b(yy, r0=0, rn=ROWS // 2 - SPLIT):
+        return xblock(yy, 1, r0, rn, x * 1024, 1024)
+
+    def x3(yy, qx, r0=0, rn=SPLIT):
+        return xblock(yy, 0, r0, rn, qx * 1024, 1024)
+
+    def x4(qx, i, r0=0, rn=ROWS // 2 - SPLIT):
+        return xblock(first if i == 0 else 1 - first, 1, r0, rn, qx * 1024, 1024)
+
+    def x3send(i, qx):
+        for d, q in (("m", yp), ("p", ym)):
+            post.send(("x3" + d, i), x3(y, qx), x3(y, qx), at(x, q, z, c), own)
+
+    def x4send(i, cond):
+        for d, q in (("m", xp), ("p", xm)):
+            post.send(("x4" + d, i), x4(x, i), x4(x, i), at(q, y, z, c), cond)
+
+    for name, half, size in (("x1", 0, SPLIT), ("x2", 1, ROWS // 2 - SPLIT)):
+        post.recv(name + "s", xblock(y, half, 0, size, mine, 512), own)
+        post.recv(name + "l", xblock(y, half, 0, size, (x * 2 + 1 - c) * 512, 512), own)
+    x4send(0, own)
+    post.recv("x1m", x1(xm), own)
+    post.send("x1m2", x1(xm, 0, near), x1(xm, 0, near), at(xp, y, z, c), own)
+    post.recv("x1p", x1(xp), own)
+    post.send("x1p2", x1(xp, near, near), x1(xp, near, near), at(xm, y, z, c), own)
+    wfirst(1, 0)
+    post.recv("x2m", x2b(ym), cm)
+    post.send("x2m2", x2b(ym, 0, far_), x2b(ym, 0, far_), at(x, yp, z, c), cm)
+    post.recv("x2p", x2b(yp), cp)
+    post.send("x2p2", x2b(yp, far_, far_), x2b(yp, far_, far_), at(x, ym, z, c), cp)
+    x4send(0, other)
+    x4send(1, own)
+    x3send(0, x)
+    x3send(1, xm)
+    x3send(2, xp)
+    zstep(1, (0,), 0)
+    post.recv("x1m2", x1(x2, 0, near), own)
+    post.recv("x1p2", x1(x2, near, near), own)
+    x3send(3, x2)
+    zstep(1, (1,), 0)
+    post.recv("x2m2", x2b(y2, 0, far_), c2)
+    post.recv("x2p2", x2b(y2, far_, far_), c2)
+    x4send(1, other)
     ostart(True)
     ostart(False)
     post.send("dec", decp, dec, partner, own)
 
-    def zstep(r, parts=(0, 1)):
-        for i in parts:
-            for d in ("m", "p"):
-                zz = (z - r) % 8 if d == "m" else (z + r) % 8
-                post.recv(("z", d, r, i), wrows(zz, i))
-                if r < 3:
-                    zsend(zz, i, r + 1, d)
-                else:
-                    zsend(zz, i, 4, d, 0 if d == "m" else 64, 64)
-                zpass(zz, i, -r % 8 if d == "m" else r)
+    def x3pass(i, qx):
+        post.recv(("x3m", i), x3(ym, qx), cm)
+        ref = x3(ym, qx, 0, near)
+        post.send(("x3m2", i), ref, ref, at(x, yp, z, c), cm)
+        post.recv(("x3p", i), x3(yp, qx), cp)
+        ref = x3(yp, qx, near, near)
+        post.send(("x3p2", i), ref, ref, at(x, ym, z, c), cp)
+
+    def x4pass(i):
+        post.recv(("x4m", i), x4(xm, i))
+        ref = x4(xm, i, 0, far_)
+        post.send(("x4m2", i), ref, ref, at(xp, y, z, c))
+        post.recv(("x4p", i), x4(xp, i))
+        ref = x4(xp, i, far_, far_)
+        post.send(("x4p2", i), ref, ref, at(xm, y, z, c))
 
     def ostep(r, i):
         for d in ("m", "p"):
@@ -265,30 +318,29 @@
                 osend(zz, i, r + 1, d)
             opass(zz, i, -r % 8 if d == "m" else r)
 
-    zstep(1)
-    post.recv(("x3m", 0), xblock(ym, 0, 0, 64, 0, 4096), cm)
-    ref = xblock(ym, 0, 0, 64, 0, 4096)
-    post.send("x3m2", ref, ref, at(x, yp, z, c), cm)
-    post.recv(("x3p", 1), xblock(yp, 0, 64, 64, 0, 4096), cp)
-    ref = xblock(yp, 0, 64, 64, 0, 4096)
-    post.send("x3p2", ref, ref, at(x, ym, z, c), cp)
-    post.recv(("x4m", 0), x4(xm, 0))
-    post.send("x4m2", x4(xm, 0), x4(xm, 0), at(xp, y, z, c))
-    post.recv(("x4p", 1), x4(xp, 1))
-    post.send("x4p2", x4(xp, 1), x4(xp, 1), at(xm, y, z, c))
-    zstep(2)
+    x4pass(0)
+    x3pass(0, x)
+    zstep(2, (0,), 0)
+    x3pass(1, xm)
+    zstep(2, (1,), 0)
+    wfirst(0, 1)
+    wfirst(1, 1)
+    x3pass(2, xp)
+    x4pass(1)
+    zstep(3, (0,), 0)
+    x3pass(3, x2)
+    zstep(3, (1,), 0)
     post.recv("o", wo.at[:, cols_at((z * 4 + 2 * c) * 128, 256)])
-    zstep(3, (0,))
-    post.recv(("x3m", 1), xblock(ym, 0, 64, 64, 0, 4096), cm)
-    post.recv(("x3p", 0), xblock(yp, 0, 0, 64, 0, 4096), cp)
-    post.recv("x3m2", xblock(y2, 0, 0, 64, 0, 4096), c2)
-    post.recv("x3p2", xblock(y2, 0, 64, 64, 0, 4096), c2)
-    post.recv(("x4m", 1), x4(xm, 1))
-    post.recv(("x4p", 0), x4(xp, 0))
-    post.recv("x4m2", x4(x2, 0))
-    post.recv("x4p2", x4(x2, 1))
+    for i, qx in enumerate((x, xm, xp, x2)):
+        post.recv(("x3m2", i), x3(y2, qx, 0, near), c2)
+        post.recv(("x3p2", i), x3(y2, qx, near, near), c2)
+    for i in (0, 1):
+        post.recv(("x4m2", i), x4(x2, i, 0, far_))
+        post.recv(("x4p2", i), x4(x2, i, far_, far_))
     for name, ref in (("gain", gain), ("cos", cosine), ("sin", sine), ("base", base), ("dk", dk), *((("v", i), pv.at[i]) for i in range(5))):
         post.recv(name, ref)
+
+    zstep(1, (0, 1), 1)
 
     @pl.loop(0, ROWS // 128)
     def _(i):
@@ -302,48 +354,31 @@
             cols = slice(k * 128, k * 128 + 128)
             nrm[rows, cols] = (xg[rows, cols].astype(F32) * scale * gain[:, cols]).astype(BF)
 
-    zstep(3, (1,))
+    def projects(p, *rels):
+        for rel in rels:
+            zz = (z + rel) % 8
+            for i in (0, 1):
+                sub = 1 - first if i == 0 else first
+                for r0, rn in ((0, 64), (64, 64)) if rel == 4 else ((0, 128),):
+                    row = (zz * 4 + 2 * (1 - c) + sub) * 128 + r0
+                    post.recv(("zp", p, rel, i, r0), wt.at[rows_at(row, rn), group_cols[p]])
+            cols = slice(512 * p, 512 + 256 * p)
+            value = dot(nrm[:, cols_at(zz * 512, 512)], wt[rows_at(zz * 512, 512), cols])
+            acc[:, cols] = value if rel == 0 else acc[:, cols] + value
+
     for i in (0, 1):
-        for d in ("m", "p"):
-            osend(z, i, 1, d)
-    for i in (0, 1):
-        opass(z, i, 0)
-
-    def zpassed(rel):
-        zz = (z + rel) % 8
-        for i in (0, 1):
-            sub = 1 - first if i == 0 else first
-            for r0, rn in ((0, 64), (64, 64)) if rel == 4 else ((0, 128),):
-                row = (zz * 4 + 2 * (1 - c) + sub) * 128 + r0
-                post.recv(("zp", rel, i, r0), wt.at[rows_at(row, rn), :])
-
-    def project(rel):
-        start = ((z + rel) % 8) * 512
-        return dot(nrm[:, cols_at(start, 512)], wt[rows_at(start, 512), :])
-
-    far = (z + 4) % 8
-
-    def projects(*rels):
-        for rel in rels:
-            zpassed(rel)
-            acc[...] = project(rel) if rel == 0 else acc[...] + project(rel)
-
-    projects(0, 1, 7, 2, 6)
-    for i in (0, 1):
-        for d, r0 in (("m", 0), ("p", 64)):
-            post.recv(("z", d, 4, i), wrows(far, i, r0, 64))
-            zpass(far, i, 4, r0, 64)
-        projects(3 if i == 0 else 5)
-    ostep(1, 0)
+        zfar(i, 0)
+    projects(0, 0, 1, 7)
+    zstep(2, (0, 1), 1)
+    projects(0, 2, 6, 3)
     post.recv("dec", dec, other)
 
     @pl.when(own)
     def _():
         dec[...] = decp[...]
 
-    zpassed(4)
-    proj = (acc[...] + project(4)).astype(BF)
-    ostep(1, 1)
+    projects(0, 5, 4)
+    proj = acc[:, 0:512].astype(BF)
     cb, sb = base[n][:, 0:128], base[n][:, 128:256]
     cosine[...], sine[...] = cosine[...] * cb - sine[...] * sb, sine[...] * cb + cosine[...] * sb
 
@@ -351,8 +386,8 @@
         wide = rows.astype(F32)
         return (wide * cosine[...] + pltpu.roll(wide, 64, axis=1) * sine[...]).astype(BF)
 
-    keys, values = turn(proj[:, 128:256]), proj[:, 256:384]
-    us[...] = (proj[:, 512:640].astype(F32) * jax.nn.sigmoid(proj[:, 640:768].astype(F32))).astype(BF)
+    keys, values = turn(proj[:, 0:128]), proj[:, 128:256]
+    us[...] = (proj[:, 256:384].astype(F32) * jax.nn.sigmoid(proj[:, 384:512].astype(F32))).astype(BF)
     after, before = (n + 1) % 16, (n + 15) % 16
     post.send("ht", us.at[pl.ds(ROWS - 16, 16), :], halo.at[0], at(x, y, after // 2, after % 2))
     post.send("hh", us.at[pl.ds(0, 16), :], halo.at[1], at(x, y, before // 2, before % 2))
@@ -362,20 +397,7 @@
     st[0] = dot((wide * jnp.exp(lb * place_)).astype(BF), values, ((0,), (0,))).astype(BF)
     st[1] = dot((wide * jnp.exp(lf * (ROWS - 1.0 - place_))).astype(BF), values, ((0,), (0,))).astype(BF)
     post.send("sp", st, sp, partner)
-    queries = turn(proj[:, 0:128])
-    gs[...] = proj[:, 384:512]
-    qs[...] = queries
-    f1, b1 = lf[:, 0:1], lb[:, 0:1]
-    for i in range(ROWS // 128):
-        rows = slice(i * 128, i * 128 + 128)
-        gap = (
-            lax.broadcasted_iota(jnp.int32, (128, ROWS), 0)
-            + i * 128
-            - lax.broadcasted_iota(jnp.int32, (128, ROWS), 1)
-        ).astype(F32)
-        decay = jnp.exp(jnp.where(gap >= 0, f1 * gap, -b1 * gap))
-        scores = dot(queries[rows], keys, ((1,), (1,))) * decay
-        inner[rows, :] = dot(scores.astype(BF), values)
+    zstep(3, (0, 1), 1)
     post.recv("sp", sp)
     span = jnp.exp(jnp.where(c == 1, lf, lb) * float(ROWS))
     chip[...] = (st[c].astype(F32) + span * sp[c].astype(F32)).astype(BF)
@@ -385,7 +407,11 @@
 
     for dz, q in line:
         post.send(("st", dz), chip, sg.at[z], at(x, y, q, c), meant(z, q))
-    ostep(2, 0)
+    for i in (0, 1):
+        for d in ("m", "p"):
+            osend(z, i, 1, d)
+    for i in (0, 1):
+        opass(z, i, 0)
 
     post.recv("ht", halo.at[0])
     post.recv("hh", halo.at[1])
@@ -402,19 +428,39 @@
         square = jnp.sum(filtered * filtered, axis=1, keepdims=True)
         tile = jnp.where(lane == 0, total, jnp.where(lane == 1, square, 0.0))
         stat[:, i * 128 : i * 128 + 128] = tile.T[0:8, :]
-    ostep(2, 1)
     me = x * 4 + y
     for i in range(4):
         for j in range(4):
             if i or j:
                 post.send("stats", stat, stats.at[me], at((x + i) % 4, (y + j) % 4, z, c))
     stats[pl.ds(me, 1)] = stat[...][None]
+    projects(1, 0, 1, 7, 2, 6)
+    for i in (0, 1):
+        zfar(i, 1)
+    projects(1, 3, 5)
+    projects(1, 4)
+    proj = acc[:, 512:768].astype(BF)
+    queries = turn(proj[:, 0:128])
+    gs[...] = proj[:, 128:256]
+    qs[...] = queries
+    f1, b1 = lf[:, 0:1], lb[:, 0:1]
+    for i in range(ROWS // 128):
+        rows = slice(i * 128, i * 128 + 128)
+        gap = (
+            lax.broadcasted_iota(jnp.int32, (128, ROWS), 0)
+            + i * 128
+            - lax.broadcasted_iota(jnp.int32, (128, ROWS), 1)
+        ).astype(F32)
+        decay = jnp.exp(jnp.where(gap >= 0, f1 * gap, -b1 * gap))
+        scores = dot(queries[rows], keys, ((1,), (1,))) * decay
+        inner[rows, :] = dot(scores.astype(BF), values)
+    ostep(1, 0)
+    ostep(1, 1)
     for dz, q in line:
         source = (z - dz) % 8
         slot = sg.at[source]
         post.recv(("st", dz), slot, meant(source, z))
         post.send(("ss", dz), slot, slot, partner, meant(source, z))
-    ostep(3, 0)
     sg[pl.ds(z, 1)] = jnp.zeros((1, 128, 128), BF)
     for dz, q in line:
         source = (z - dz) % 8
@@ -439,7 +485,6 @@
     scaled = centered * lax.rsqrt(variance + EPS) * pv[3] + pv[4]
     both[:, 0:128] = (jax.nn.silu(gs[...].astype(F32)) * scaled).astype(BF)
 
-    ostep(3, 1)
     post.recv("stats", stats.at[pl.ds(0, 15)])
     total = stats[0]
     for j in range(1, 16):
@@ -462,7 +507,6 @@
 
     to_xp, to_xm = at(xp, y, z, c), at(xm, y, z, c)
     c1p, c1m = cp, cm
-    right = pl.ds(2560, 1536)
     groups = (pl.ds(0, 1536), pl.ds(1536, 1024))
 
     def add(a, b):
@@ -509,68 +553,93 @@
                 value = value + ua[q, :, piece].astype(F32)
             out[:, cols_at(((z + ORDER[k]) % 8) * 512, 512)] = value.astype(BF)
 
-    def pb(yy, q0, k):
-        return part.at[yy % 2, pl.ds(q0, 2), k, :, right]
+    bgroups = ((0, 1024), (1024, 512))
+
+    def pb(yy, q0, k, g):
+        return part.at[yy % 2, pl.ds(q0, 2), k, :, pl.ds(2560 + bgroups[g][0], bgroups[g][1])]
+
+    def bfirst(g):
+        cols, size = pl.ds(*bgroups[g]), bgroups[g][1]
+        whole = pl.ds(2560 + bgroups[g][0], size)
+        for k in (0, 1):
+            post.send(("b2m", g), pb(y2, 0, k, g), b2m.at[k, :, :, cols], at(x, yp, z, c), c2)
+            post.send(("b2p", g), pb(y2, 2, k, g), b2p.at[k, :, :, cols], at(x, ym, z, c), c2)
+        for k in (0, 1):
+            post.send(("bm1", g), pb(yp, 2, k, g), bm.at[pl.ds(2, 2), :, cols], at(x, yp, z, k), c1p)
+            post.send(("bp0", g), pb(ym, 0, k, g), bp.at[pl.ds(0, 2), :, cols], at(x, ym, z, k), c1m)
+        post.send(("bo", g), part.at[y % 2, :, 1 - c, :, whole], bo.at[:, :, cols], partner, own)
+
+        @pl.when(own)
+        def _():
+            bo[:, :, cols] = part[y % 2, :, c, :, whole]
+
+    def bsecond(g):
+        cols = pl.ds(*bgroups[g])
+        whole = pl.ds(2560 + bgroups[g][0], bgroups[g][1])
+        for name, ref, yy, q0, slot, cond, qy, dst in (
+            ("b2m", b2m, yp, 0, 0, c1p, yp, bm),
+            ("b2p", b2p, ym, 2, 1, c1m, ym, bp),
+        ):
+            post.recv((name, g), ref.at[:, :, :, cols], cond)
+
+            @pl.when(cond)
+            def _():
+                for k in (0, 1):
+                    tb[slot, k, :, :, cols] = add(ref[k, :, :, cols], part[yy % 2, q0 : q0 + 2, k, :, whole])
+
+            for k in (0, 1):
+                src = tb.at[slot, k, :, :, cols]
+                post.send((name, "sum", g), src, dst.at[pl.ds(q0, 2), :, cols], at(x, qy, z, k), cond)
+
+    def bthird(g):
+        cols = pl.ds(*bgroups[g])
+        post.recv(("bm1", g), bm.at[pl.ds(2, 2), :, cols])
+        post.recv(("bp0", g), bp.at[pl.ds(0, 2), :, cols])
+        post.recv(("bo", g), bo.at[:, :, cols], other)
+        post.recv(("b2m", "sum", g), bm.at[pl.ds(0, 2), :, cols])
+        post.recv(("b2p", "sum", g), bp.at[pl.ds(2, 2), :, cols])
+        for q in range(4):
+            value = bm[q, :, cols].astype(F32) + bp[q, :, cols].astype(F32)
+            v[q, :, cols] = (value + bo[q, :, cols].astype(F32)).astype(BF)
+        for q in (x2, xp, xm):
+            post.send(("vb", g), v.at[q, :, cols], vb.at[x, :, cols], at(q, y, z, c))
+        vb[pl.ds(x, 1), :, cols] = v[pl.ds(x, 1), :, cols]
+
+    def blast(g):
+        cols = pl.ds(*bgroups[g])
+        post.recv(("vb", g), vb.at[pl.ds(0, 3), :, cols])
+        for k in range(bgroups[g][0] // 512, sum(bgroups[g]) // 512):
+            piece = slice(k * 512, k * 512 + 512)
+            value = vb[0, :, piece].astype(F32)
+            for q in (1, 2, 3):
+                value = value + vb[q, :, piece].astype(F32)
+            out[:, cols_at(((z + ORDER[k + 5]) % 8) * 512, 512)] = value.astype(BF)
 
     out_part((0, 1, 2))
     afirst(0)
+    ostep(2, 0)
+    ostep(2, 1)
     out_part((3, 4))
     afirst(1)
     for i in (0, 1):
+        ostep(3, i)
+    out_part((5, 6))
+    bfirst(0)
+    asecond(0)
+    for i in (0, 1):
         ostep(4, i)
-    out_part((5, 6, 7))
-    for k in (0, 1):
-        post.send("b2m", pb(y2, 0, k), b2m.at[k], at(x, yp, z, c), c2)
-        post.send("b2p", pb(y2, 2, k), b2p.at[k], at(x, ym, z, c), c2)
-    for k in (0, 1):
-        post.send("bm1", pb(yp, 2, k), bm.at[pl.ds(2, 2)], at(x, yp, z, k), c1p)
-        post.send("bp0", pb(ym, 0, k), bp.at[pl.ds(0, 2)], at(x, ym, z, k), c1m)
-    post.send("bo", part.at[y % 2, :, 1 - c, :, right], bo, partner, own)
-    asecond(0)
+    out_part((7,))
+    bfirst(1)
+    bsecond(0)
     asecond(1)
-    post.recv("b2m", b2m, c1p)
-
-    @pl.when(c1p)
-    def _():
-        for k in (0, 1):
-            tb[0, k] = add(b2m[k], part[yp % 2, 0:2, k, :, right])
-
-    for k in (0, 1):
-        post.send("bm0", tb.at[0, k], bm.at[pl.ds(0, 2)], at(x, yp, z, k), c1p)
-    post.recv("b2p", b2p, c1m)
-
-    @pl.when(c1m)
-    def _():
-        for k in (0, 1):
-            tb[1, k] = add(b2p[k], part[ym % 2, 2:4, k, :, right])
-
-    for k in (0, 1):
-        post.send("bp1", tb.at[1, k], bp.at[pl.ds(2, 2)], at(x, ym, z, k), c1m)
-
-    @pl.when(own)
-    def _():
-        bo[...] = part[y % 2, :, c, :, right]
-
+    bsecond(1)
+    bthird(0)
     athird(0)
-    post.recv("bm1", bm.at[pl.ds(2, 2)])
-    post.recv("bp0", bp.at[pl.ds(0, 2)])
-    post.recv("bo", bo, other)
-    post.recv("bm0", bm.at[pl.ds(0, 2)])
-    post.recv("bp1", bp.at[pl.ds(2, 2)])
-    for q in range(4):
-        v[q] = (bm[q].astype(F32) + bp[q].astype(F32) + bo[q].astype(F32)).astype(BF)
-    for q in (x2, xp, xm):
-        post.send("vb", v.at[q], vb.at[x], at(q, y, z, c))
-    vb[pl.ds(x, 1)] = v[pl.ds(x, 1)]
+    bthird(1)
     athird(1)
+    blast(0)
     alast(0)
-    post.recv("vb", vb.at[pl.ds(0, 3)])
-    for k in (5, 6, 7):
-        piece = slice((k - 5) * 512, (k - 5) * 512 + 512)
-        value = vb[0, :, piece].astype(F32)
-        for q in (1, 2, 3):
-            value = value + vb[q, :, piece].astype(F32)
-        out[:, cols_at(((z + ORDER[k]) % 8) * 512, 512)] = value.astype(BF)
+    blast(1)
     alast(1)
     post.finish()
 
@@ -616,6 +685,10 @@
         in_specs=[HBM] * 19 + [SM] * 2,
         out_specs=VM,
         scratch_shapes=[
+            pltpu.VMEM((256, 512), BF),
+            pltpu.VMEM((6, 128, 256), BF),
+            pltpu.VMEM((256, 128), BF),
+            pltpu.VMEM((256, 128), BF),
             pltpu.VMEM((ROWS, 4096), BF),
             pltpu.VMEM((ROWS, 4096), BF),
             pltpu.VMEM((4096, 768), BF),
@@ -659,20 +732,20 @@
             narrow(2, 2, 2, 32),
             narrow(4, 32),
             narrow(4, 32),
-            pltpu.SemaphoreType.DMA((230,)),
-            pltpu.SemaphoreType.DMA((180,)),
+            pltpu.SemaphoreType.DMA((340,)),
+            pltpu.SemaphoreType.DMA((260,)),
         ],
         compiler_params=pltpu.CompilerParams(
             collective_id=0, has_side_effects=True, vmem_limit_bytes=67043328
         ),
     )(
         hidden_states,
-        query_weight,
         key_weight,
         value_weight,
-        output_gate_weight,
         unit_input_weight,
         unit_gate_weight,
+        query_weight,
+        output_gate_weight,
         retention_out_weight,
         convolution_out_weight,
         depth_kernel,

time: 100 us -> 97 us (0.970)
  Pallas kernels: 98.4 us -> 95.2 us
    pallas_call x1, Pallas kernels: 98.4 us -> 95.2 us  [shards(): pl.pallas_call(mixer_kernel, name='mixer', out_shape=jax.ShapeDtypeStruct...]
where the time goes in v4:
time: 97 us; the launch traced here: 96.9 us
  Pallas kernels  95.2 us (98%)
  local copies, waits for them, and re-layouts  1.67 us (2%)
    pallas_call x1, Pallas kernels, shards(): pl.pallas_call(mixer_kernel, name='mixer', out_shape=jax.ShapeDtypeStruct...  95.2 us

profile of v4, /device:TPU:1, one launch (start us, length us, event | category | flops | bytes accessed | tf_op | source)
XLA Modules:
  0.0 96.9 jit_solution(12159588639364354674)
XLA Ops:
  0.0 95.2 %mixer.1 = bf16[32,4096]{1,0:T(8,128)(2,1)} custom-call(bf16[256,512]{1,0:T(8,128)(2,1)} %xin.1, bf16[128,256]{1,0:T(8,128)(2,1)} %w0.1, bf16[128,256]{1,0:T(8,128)(2,1)} %w1.1, bf16[128,256]{1,0:T(8,128)(2,1)} %w2.1, bf16[128,256]{1,0:T(8,128)(2,1)} %w3.1, bf16[128,256]{1,0:T(8,128)(2,1)} %w4.1, bf16[128,256]{1,0:T(8,128)(2,1)} %w5.1, bf16[256,128]{1,0:T(8,128)(2,1)} %wr.1, ...), custom_call_target="tpu_custom_call" | custom-call | tf_op jit(solution)/shard_map/mixer/pallas_call | solution.py:681
  95.2 1.7 %copy.23 = bf16[32,4096]{1,0:T(8,128)(2,1)} copy(bf16[32,4096]{1,0:T(8,128)(2,1)} %mixer.1) | data formatting | bytes 524288

commit v5 on v4

--- a/solution.py
+++ b/solution.py
@@ -318,9 +318,9 @@
                 osend(zz, i, r + 1, d)
             opass(zz, i, -r % 8 if d == "m" else r)
 
+    zstep(2, (0,), 0)
     x4pass(0)
     x3pass(0, x)
-    zstep(2, (0,), 0)
     x3pass(1, xm)
     zstep(2, (1,), 0)
     wfirst(0, 1)
@@ -507,7 +507,7 @@
 
     to_xp, to_xm = at(xp, y, z, c), at(xm, y, z, c)
     c1p, c1m = cp, cm
-    groups = (pl.ds(0, 1536), pl.ds(1536, 1024))
+    groups = (pl.ds(0, 1536), pl.ds(1536, 512))
 
     def add(a, b):
         return (a.astype(F32) + b.astype(F32)).astype(BF)
@@ -553,14 +553,14 @@
                 value = value + ua[q, :, piece].astype(F32)
             out[:, cols_at(((z + ORDER[k]) % 8) * 512, 512)] = value.astype(BF)
 
-    bgroups = ((0, 1024), (1024, 512))
+    bgroups = ((0, 512), (512, 1024), (1536, 512))
 
     def pb(yy, q0, k, g):
-        return part.at[yy % 2, pl.ds(q0, 2), k, :, pl.ds(2560 + bgroups[g][0], bgroups[g][1])]
+        return part.at[yy % 2, pl.ds(q0, 2), k, :, pl.ds(2048 + bgroups[g][0], bgroups[g][1])]
 
     def bfirst(g):
         cols, size = pl.ds(*bgroups[g]), bgroups[g][1]
-        whole = pl.ds(2560 + bgroups[g][0], size)
+        whole = pl.ds(2048 + bgroups[g][0], size)
         for k in (0, 1):
             post.send(("b2m", g), pb(y2, 0, k, g), b2m.at[k, :, :, cols], at(x, yp, z, c), c2)
             post.send(("b2p", g), pb(y2, 2, k, g), b2p.at[k, :, :, cols], at(x, ym, z, c), c2)
@@ -575,7 +575,7 @@
 
     def bsecond(g):
         cols = pl.ds(*bgroups[g])
-        whole = pl.ds(2560 + bgroups[g][0], bgroups[g][1])
+        whole = pl.ds(2048 + bgroups[g][0], bgroups[g][1])
         for name, ref, yy, q0, slot, cond, qy, dst in (
             ("b2m", b2m, yp, 0, 0, c1p, yp, bm),
             ("b2p", b2p, ym, 2, 1, c1m, ym, bp),
@@ -613,7 +613,7 @@
             value = vb[0, :, piece].astype(F32)
             for q in (1, 2, 3):
                 value = value + vb[q, :, piece].astype(F32)
-            out[:, cols_at(((z + ORDER[k + 5]) % 8) * 512, 512)] = value.astype(BF)
+            out[:, cols_at(((z + ORDER[k + 4]) % 8) * 512, 512)] = value.astype(BF)
 
     out_part((0, 1, 2))
     afirst(0)
@@ -621,26 +621,30 @@
     ostep(2, 1)
     out_part((3, 4))
     afirst(1)
+    bfirst(0)
     for i in (0, 1):
         ostep(3, i)
     out_part((5, 6))
-    bfirst(0)
+    bfirst(1)
+    bsecond(0)
     asecond(0)
     for i in (0, 1):
         ostep(4, i)
     out_part((7,))
-    bfirst(1)
-    bsecond(0)
+    bfirst(2)
+    bsecond(1)
     asecond(1)
-    bsecond(1)
+    bsecond(2)
     bthird(0)
     athird(0)
     bthird(1)
     athird(1)
+    bthird(2)
     blast(0)
     alast(0)
     blast(1)
     alast(1)
+    blast(2)
     post.finish()
 
 
@@ -675,8 +679,8 @@
     convolution_out_weight,
 ):
     vectors = (depth_bias, channel_gain, channel_bias, group_gain, group_bias)
-    wide = lambda *shape: pltpu.VMEM((*shape, 2560), BF)
-    narrow = lambda *shape: pltpu.VMEM((*shape, 1536), BF)
+    wide = lambda *shape: pltpu.VMEM((*shape, 2048), BF)
+    narrow = lambda *shape: pltpu.VMEM((*shape, 2048), BF)
     small = lambda dtype: pltpu.VMEM((ROWS, 128), dtype)
     return pl.pallas_call(
         mixer_kernel,
@@ -732,8 +736,8 @@
             narrow(2, 2, 2, 32),
             narrow(4, 32),
             narrow(4, 32),
-            pltpu.SemaphoreType.DMA((340,)),
-            pltpu.SemaphoreType.DMA((260,)),
+            pltpu.SemaphoreType.DMA((360,)),
+            pltpu.SemaphoreType.DMA((280,)),
         ],
         compiler_params=pltpu.CompilerParams(
             collective_id=0, has_side_effects=True, vmem_limit_bytes=67043328

time: 97 us -> 96.5 us (level)
  no operation moved by 1% of the time
where the time goes in v5:
time: 96.5 us; the launch traced here: 96.3 us
  Pallas kernels  94.7 us (98%)
  local copies, waits for them, and re-layouts  1.67 us (2%)
    pallas_call x1, Pallas kernels, shards(): pl.pallas_call(mixer_kernel, name='mixer', out_shape=jax.ShapeDtypeStruct...  94.7 us

profile of v5, /device:TPU:1, one launch (start us, length us, event | category | flops | bytes accessed | tf_op | source)
XLA Modules:
  0.0 96.3 jit_solution(5079835818762457762)
XLA Ops:
  0.0 94.7 %mixer.1 = bf16[32,4096]{1,0:T(8,128)(2,1)} custom-call(bf16[256,512]{1,0:T(8,128)(2,1)} %xin.1, bf16[128,256]{1,0:T(8,128)(2,1)} %w0.1, bf16[128,256]{1,0:T(8,128)(2,1)} %w1.1, bf16[128,256]{1,0:T(8,128)(2,1)} %w2.1, bf16[128,256]{1,0:T(8,128)(2,1)} %w3.1, bf16[128,256]{1,0:T(8,128)(2,1)} %w4.1, bf16[128,256]{1,0:T(8,128)(2,1)} %w5.1, bf16[256,128]{1,0:T(8,128)(2,1)} %wr.1, ...), custom_call_target="tpu_custom_call" | custom-call | tf_op jit(solution)/shard_map/mixer/pallas_call | solution.py:685
  94.7 1.7 %copy.23 = bf16[32,4096]{1,0:T(8,128)(2,1)} copy(bf16[32,4096]{1,0:T(8,128)(2,1)} %mixer.1) | data formatting | bytes 524288
